TPU v7x, 128 devices: a whole 4x4x4 slice. The times are simulated.
128 devices in a mesh: ep: 128 (over z, y, x, core).
Axes of the slice: x: 4, y: 4, z: 4, core: 2. Of those that a mesh axis runs over, the one named last changes fastest.
Arguments:
- residual: bfloat16 [8192, 2048], P('ep'), may hold values from -6 to 6
- branch_in: bfloat16 [8192, 1024], P('ep'), may hold values from -6 to 6
- state_real: float32 [8192, 4096], P('ep'), may hold values from -4 to 4
- state_imag: float32 [8192, 4096], P('ep'), may hold values from -4 to 4
- decay_rate: float32 [64, 64], replicated, may hold values from 0.1 to 1
- frequency: float32 [64, 64], replicated, may hold values from 0 to 200
- log_step: float32 [64], replicated, may hold values from -4 to 0
- input_real: bfloat16 [64, 64, 16], replicated, may hold values from -1 to 1
- input_imag: bfloat16 [64, 64, 16], replicated, may hold values from -1 to 1
- output_matrix_real: bfloat16 [64, 16, 64], replicated, may hold values from -0.5 to 0.5
- output_matrix_imaginary: bfloat16 [64, 16, 64], replicated, may hold values from -0.5 to 0.5
- skip_gain: float32 [1024], replicated, may hold values from -4 to 4
- glu_value: bfloat16 [1024, 2048], replicated, may hold values from -0.1875 to 0.1875
- glu_gate: bfloat16 [1024, 2048], replicated, may hold values from -0.1875 to 0.1875
- mix_gain: float32 [2048], replicated, may hold values from 0.1 to 1.9
- moe_in_gain: float32 [2048], replicated, may hold values from 0.1 to 1.9
- moe_out_gain: float32 [2048], replicated, may hold values from 0.1 to 1.9
- routes: int32 [8192, 6], P('ep'), may hold values from 0 to 127, all different within a row; in each aligned block of 64 rows (0 to 63, 64 to 127, ...) at most 4 rows name the same one
- route_weights: float32 [8192, 6], P('ep'), may hold values from 0.05 to 0.6
- expert_gate: bfloat16 [128, 2048, 512], P('ep'), may hold values from -0.125 to 0.125
- expert_up: bfloat16 [128, 2048, 512], P('ep'), may hold values from -0.125 to 0.125
- expert_down: bfloat16 [128, 512, 2048], P('ep'), may hold values from -0.25 to 0.25
- shared_gate: bfloat16 [2048, 512], replicated, may hold values from -0.125 to 0.125
- shared_up: bfloat16 [2048, 512], replicated, may hold values from -0.125 to 0.125
- shared_down: bfloat16 [512, 2048], replicated, may hold values from -0.25 to 0.25
Outputs:
- layer_out: bfloat16 [8192, 2048], P('ep')
- next_real: float32 [8192, 4096], P('ep')
- next_imag: float32 [8192, 4096], P('ep')
Inputs may be any that keep to these rules, and one draw needn't show every extreme that they name: `routes`: among the rows of one device no expert is named more than 4 times, and in every draw some expert is named exactly 4 times by some device's rows; a token's experts are distinct.
All inputs are finite; a program needn't handle non-finite values.
Results may differ from a plain program's by a relative error of at most 0.0066.
Values may be sent and summed in bfloat16 or wider, within the bound.
A program may use at most 128 MiB of HBM per device.

v0:
```python
import jax
import jax.numpy as jnp
from jax import lax
from jax.sharding import PartitionSpec as P

norm_eps = 1e-06


def scaled_norm(row_block, norm_gain):
    return (
        row_block
        * lax.rsqrt(jnp.mean(row_block * row_block, axis=-1, keepdims=True) + norm_eps)
        * norm_gain
    )


def state_step(
    branch_in,
    state_real,
    state_imag,
    decay_rate,
    frequency,
    log_step,
    input_real,
    input_imag,
    output_matrix_real,
    output_matrix_imaginary,
    skip_gain,
):
    seq_count = branch_in.shape[0]
    group_count, state_count = decay_rate.shape
    chan_count = input_real.shape[2]
    step_size = jnp.exp(log_step)[:, None]
    magnitude = jnp.exp(-decay_rate * step_size)
    abar_re = magnitude * jnp.cos(frequency * step_size)
    abar_im = magnitude * jnp.sin(frequency * step_size)
    lam_re = -decay_rate
    denominator = lam_re * lam_re + frequency * frequency
    numer_re = abar_re - 1.0
    coef_re = (numer_re * lam_re + abar_im * frequency) / denominator
    coef_im = (abar_im * lam_re - numer_re * frequency) / denominator
    b_real = input_real.astype(jnp.float32)
    b_imag = input_imag.astype(jnp.float32)
    bbar_re = coef_re[..., None] * b_real - coef_im[..., None] * b_imag
    bbar_im = coef_re[..., None] * b_imag + coef_im[..., None] * b_real
    feed_rows = branch_in.astype(jnp.float32).reshape(seq_count, group_count, chan_count)
    forcing_real = jnp.einsum("tgc,gpc->tgp", feed_rows, bbar_re, precision=lax.Precision.HIGHEST)
    drive_im = jnp.einsum("tgc,gpc->tgp", feed_rows, bbar_im, precision=lax.Precision.HIGHEST)
    old_re = state_real.reshape(seq_count, group_count, state_count)
    old_im = state_imag.reshape(seq_count, group_count, state_count)
    fresh_real = abar_re * old_re - abar_im * old_im + forcing_real
    fresh_imaginary = abar_re * old_im + abar_im * old_re + drive_im
    state_readout = jnp.einsum(
        "ukb,krb->ukr",
        fresh_real,
        output_matrix_real.astype(jnp.float32),
        precision=lax.Precision.HIGHEST,
    ) - jnp.einsum(
        "ukb,krb->ukr",
        fresh_imaginary,
        output_matrix_imaginary.astype(jnp.float32),
        precision=lax.Precision.HIGHEST,
    )
    mixed_rows = state_readout.reshape(
        seq_count, group_count * chan_count
    ) + skip_gain * branch_in.astype(jnp.float32)
    activated = jax.nn.gelu(mixed_rows).astype(jnp.bfloat16)
    return (activated, fresh_real.reshape(seq_count, -1), fresh_imaginary.reshape(seq_count, -1))


def expert_rows(row_block, w_gate, w_up, w_down):
    gate_part = jnp.dot(row_block, w_gate, preferred_element_type=jnp.float32)
    up_part = jnp.dot(row_block, w_up, preferred_element_type=jnp.float32)
    hidden = (jax.nn.silu(gate_part) * up_part).astype(jnp.bfloat16)
    return jnp.dot(hidden, w_down, preferred_element_type=jnp.float32)


def mixer_residual(residual, activated, glu_value, glu_gate, mix_gain):
    value_part = jnp.dot(activated, glu_value, preferred_element_type=jnp.float32)
    gate_part = jnp.dot(activated, glu_gate, preferred_element_type=jnp.float32)
    branch = value_part * jax.nn.sigmoid(gate_part)
    return (residual.astype(jnp.float32) + scaled_norm(branch, mix_gain)).astype(jnp.bfloat16)


def serve_rows(
    residual, branch_in, state_real, state_imag, routes, route_weights, params, capacity
):
    (
        decay_rate,
        frequency,
        log_step,
        input_real,
        input_imag,
        output_matrix_real,
        output_matrix_imaginary,
        skip_gain,
        glu_value,
        glu_gate,
        mix_gain,
        moe_in_gain,
        moe_out_gain,
        expert_gate,
        expert_up,
        expert_down,
        shared_gate,
        shared_up,
        shared_down,
    ) = params
    activated, next_real, next_imag = state_step(
        branch_in,
        state_real,
        state_imag,
        decay_rate,
        frequency,
        log_step,
        input_real,
        input_imag,
        output_matrix_real,
        output_matrix_imaginary,
        skip_gain,
    )
    resid_mid = mixer_residual(residual, activated, glu_value, glu_gate, mix_gain)
    normed = scaled_norm(resid_mid.astype(jnp.float32), moe_in_gain).astype(jnp.bfloat16)
    seq_count, hidden_width = normed.shape
    top_count = routes.shape[1]
    expert_count = lax.axis_size("ep")
    flat_routes = routes.reshape(-1)
    assign_count = seq_count * top_count
    position = jnp.arange(assign_count, dtype=jnp.int32)
    earlier = (flat_routes[:, None] == flat_routes[None, :]) & (
        position[None, :] < position[:, None]
    )
    slot_rank = jnp.sum(earlier.astype(jnp.int32), axis=1)
    slot_index = flat_routes * capacity + slot_rank
    slot_source = (
        jnp.full((expert_count * capacity,), seq_count, jnp.int32)
        .at[slot_index]
        .set(position // top_count)
    )
    padded = jnp.concatenate([normed, jnp.zeros((1, hidden_width), jnp.bfloat16)], axis=0)
    outgoing = padded[slot_source].reshape(expert_count, capacity, hidden_width)
    received_rows = lax.all_to_all(outgoing, "ep", split_axis=0, concat_axis=0, tiled=True)
    source_count = received_rows.shape[0]
    item_count = received_rows.shape[1]
    produced = expert_rows(
        received_rows.reshape(-1, hidden_width), expert_gate[0], expert_up[0], expert_down[0]
    ).astype(jnp.bfloat16)
    returned = lax.all_to_all(
        produced.reshape(source_count, item_count, hidden_width),
        "ep",
        split_axis=0,
        concat_axis=0,
        tiled=True,
    )
    per_assign = (
        returned.reshape(-1, hidden_width)[slot_index]
        .reshape(seq_count, top_count, hidden_width)
        .astype(jnp.float32)
    )
    routed = jnp.sum(per_assign * route_weights[..., None], axis=1)
    shared = expert_rows(normed, shared_gate, shared_up, shared_down)
    combined = shared + routed
    layer_out = (resid_mid.astype(jnp.float32) + scaled_norm(combined, moe_out_gain)).astype(
        jnp.bfloat16
    )
    return (layer_out, next_real, next_imag)


def per_device(
    residual,
    branch_in,
    state_real,
    state_imag,
    decay_rate,
    frequency,
    log_step,
    input_real,
    input_imag,
    output_matrix_real,
    output_matrix_imaginary,
    skip_gain,
    glu_value,
    glu_gate,
    mix_gain,
    moe_in_gain,
    moe_out_gain,
    routes,
    route_weights,
    expert_gate,
    expert_up,
    expert_down,
    shared_gate,
    shared_up,
    shared_down,
):
    params = (
        decay_rate,
        frequency,
        log_step,
        input_real,
        input_imag,
        output_matrix_real,
        output_matrix_imaginary,
        skip_gain,
        glu_value,
        glu_gate,
        mix_gain,
        moe_in_gain,
        moe_out_gain,
        expert_gate,
        expert_up,
        expert_down,
        shared_gate,
        shared_up,
        shared_down,
    )
    seq_dev = residual.shape[0]
    capacity = max(2, 4 * seq_dev * routes.shape[1] // (3 * lax.axis_size("ep")))
    return serve_rows(
        residual, branch_in, state_real, state_imag, routes, route_weights, params, capacity
    )


def solution(mesh):
    return jax.shard_map(
        per_device,
        mesh=mesh,
        in_specs=(
            P("ep", None),
            P("ep", None),
            P("ep", None),
            P("ep", None),
            P(),
            P(),
            P(),
            P(),
            P(),
            P(),
            P(),
            P(),
            P(),
            P(),
            P(),
            P(),
            P(),
            P("ep", None),
            P("ep", None),
            P("ep", None, None),
            P("ep", None, None),
            P("ep", None, None),
            P(),
            P(),
            P(),
        ),
        out_specs=(P("ep", None), P("ep", None), P("ep", None)),
        check_vma=False,
    )
```

profile of v0, /device:TPU:1, one launch (start us, length us, event | category | flops | bytes accessed | tf_op | source)
XLA Modules:
  0.0 162.2 jit_solution(14175542040861350788)
XLA Ops:
  0.6 0.0 copy-start
  0.7 0.8 broadcast_multiply_fusion
  1.5 0.8 copy.56
  2.3 0.7 exp.17
  2.9 1.1 copy.51
  4.0 3.2 %copy.49 = f32[64,4096]{0,1:T(8,128)} copy(f32[64,4096]{1,0:T(8,128)} %param.27) | data formatting | bytes 2097152 | tf_op args[2]
  7.2 3.2 %copy.50 = f32[64,4096]{0,1:T(8,128)} copy(f32[64,4096]{1,0:T(8,128)} %param.28) | data formatting | bytes 2097152 | tf_op args[3]
  10.4 0.0 copy-done.11
  10.4 0.0 copy-done.12
  10.4 0.2 add_divide_fusion
  10.6 0.0 copy-done.5
  10.6 0.0 copy-done.6
  10.6 0.0 copy-start.1
  10.6 0.0 copy-start.2
  10.7 6.0 %bitcast_add_fusion = f32[64,64,64]{0,2,1:T(8,128)} fusion(f32[64,64,64]{0,2,1:T(8,128)} %bitcast.45, f32[64,64,64]{0,2,1:T(8,128)} %bitcast.47, bf16[64,64,16]{0,2,1:T(8,128)(2,1)S(1)} %bitcast.51, f32[64,64]{1,0:T(8,128)S(1)} %get-tuple-element.17, f32[64,64]{1,0:T(8,128)S(1)} %get-tuple-element.15, bf16[64,64,16]{1,2,0:T(8,128)(2,1)S(1)} %copy-done.5, ...), kind=kOutput, calls=%fused_computation.16 | convolution fusion | flops 51707904 | bytes 3604480 | tf_op jit(solution)/shard_map/tgc,gpc->tgp/dot_general | solution.py:48
  16.6 0.0 copy-done.1
  16.7 0.0 copy-done.2
  16.7 4.1 %bitcast_add_fusion.1 = f32[64,64,64]{0,2,1:T(8,128)} fusion(f32[64,64,64]{0,2,1:T(8,128)S(1)} %bitcast.48, f32[64,64,64]{0,2,1:T(8,128)S(1)} %bitcast.46, bf16[64,64,16]{0,2,1:T(8,128)(2,1)S(1)} %bitcast.52, f32[64,64]{1,0:T(8,128)S(1)} %get-tuple-element.17, f32[64,64]{1,0:T(8,128)S(1)} %get-tuple-element.15, bf16[64,64,16]{1,2,0:T(8,128)(2,1)S(1)} %copy-done.5, ...), kind=kOutput, calls=%fused_computation.17 | convolution fusion | flops 51707904 | bytes 3604480 | tf_op jit(solution)/shard_map/tgc,gpc->tgp/dot_general | solution.py:47
  20.7 0.1 copy.55
  20.8 0.1 mul.272
  21.0 0.1 eq.15
  21.1 0.2 convert_reduce_fusion
  21.4 2.9 %scatter_custom_fusion = s32[512]{0:T(512)S(1)} fusion(s32[384]{0:T(512)S(1)} %fusion.48, s32[384]{0:T(512)S(1)} %add_select_fusion, s32[]{:T(128)} %constant.14.clone.1), kind=kCustom, calls=%fused_computation.81 | custom fusion | bytes 2052 | tf_op jit(solution)/shard_map/scatter | solution.py:138
  24.3 0.0 copy-start.3
  24.3 0.0 copy-done.9
  24.3 2.8 %fusion.53 = f32[64,64,16]{1,2,0:T(8,128)S(1)} fusion(f32[64,64,64]{0,2,1:T(8,128)} %bitcast_add_fusion.1, bf16[64,16,64]{2,1,0:T(8,128)(2,1)S(1)} %copy-done.9), kind=kOutput, calls=%fused_computation.88 | convolution fusion | flops 50331648 | bytes 1441792 | tf_op jit(solution)/shard_map/ukb,krb->ukr/dot_general | solution.py:53
  27.2 0.0 copy-done.10
  27.2 0.0 copy-done.3
  27.2 0.0 copy-start.7
  27.2 0.0 copy-start.16
  27.2 1.1 convolution_subtract_fusion
  28.3 0.2 copy.54
  28.5 0.0 copy-done.7
  28.5 0.0 copy-done.16
  28.5 0.1 fusion.34
  28.7 0.0 copy-start.4
  28.7 3.2 %fusion.2 = f32[64,2048]{1,0:T(8,128)S(1)} fusion(bf16[64,1024]{1,0:T(8,128)(2,1)S(1)} %fusion.34, bf16[1024,2048]{1,0:T(8,128)(2,1)} %param.38), kind=kOutput, calls=%fused_computation.10 | convolution fusion | flops 268828672 | bytes 4849664 | tf_op jit(solution)/shard_map/dot_general | solution.py:80
  31.9 0.2 copy-done.4
  32.1 1.0 multiply_reduce_fusion.2
  33.1 0.0 copy-done.8
  33.1 0.3 fusion.22
  33.4 0.0 copy-done.14
  33.4 0.1 fusion.24
  33.6 3.3 %gather_fusion = bf16[512,2048]{1,0:T(8,128)(2,1)} fusion(bf16[65,2048]{1,0:T(8,128)(2,1)S(1)} %concatenate.3, s32[1024]{0:T(1024)S(1)} %pad_clamp_fusion.1), kind=kCustom, calls=%fused_computation | custom fusion | bytes 4196352 | tf_op jit(solution)/shard_map/gather | solution.py:141
  36.9 4.1 %reshape.108 = bf16[128,4,2048]{2,1,0:T(4,128)(2,1)} reshape(bf16[512,2048]{1,0:T(8,128)(2,1)} %gather_fusion) | data formatting | bytes 4194304 | tf_op jit(solution)/shard_map/reshape | solution.py:141
  41.0 42.1 %all_to_all.10 = bf16[128,4,2048]{2,1,0:T(4,128)(2,1)} all-to-all(bf16[128,4,2048]{2,1,0:T(4,128)(2,1)} %reshape.108), channel_id=1, replica_groups=mesh['ep'=128] {'ep'}, dimensions={0} | all-to-all | bytes 4194304 | tf_op jit(solution)/shard_map/all_to_all | solution.py:142
  83.1 4.0 %reshape.109 = bf16[512,2048]{1,0:T(8,128)(2,1)} reshape(bf16[128,4,2048]{2,1,0:T(4,128)(2,1)} %all_to_all.10) | data formatting | bytes 4194304 | tf_op jit(solution)/shard_map/reshape | solution.py:146
  87.0 4.4 %fusion.6 = f32[512,512]{1,0:T(8,128)} fusion(bf16[512,2048]{1,0:T(8,128)(2,1)} %reshape.109, bf16[1,2048,512]{2,1,0:T(8,128)(2,1)} %param.44), kind=kOutput, calls=%fused_computation.14 | convolution fusion | flops 1073741824 | bytes 5242880 | tf_op jit(solution)/shard_map/dot_general | solution.py:72
  91.5 6.3 %convolution_convert_fusion = bf16[512,2048]{1,0:T(8,128)(2,1)} fusion(bf16[1,512,2048]{2,1,0:T(8,128)(2,1)S(1)} %copy-done, bf16[512,2048]{1,0:T(8,128)(2,1)} %reshape.109, bf16[1,2048,512]{2,1,0:T(8,128)(2,1)} %param.45, f32[512,512]{1,0:T(8,128)} %fusion.6), kind=kOutput, calls=%fused_computation.4 | convolution fusion | flops 2150105088 | bytes 9437184 | tf_op jit(solution)/shard_map/dot_general | solution.py:75
  97.7 4.2 %reshape.110 = bf16[128,4,2048]{2,1,0:T(4,128)(2,1)} reshape(bf16[512,2048]{1,0:T(8,128)(2,1)} %convolution_convert_fusion) | data formatting | bytes 4194304 | tf_op jit(solution)/shard_map/reshape | solution.py:149
  101.9 5.6 %all-to-all-start.1 = ((bf16[128,4,2048]{2,1,0:T(4,128)(2,1)}), bf16[128,4,2048]{2,1,0:T(4,128)(2,1)}, u32[]{:S(2)}, u32[]{:S(2)}) async-start(bf16[128,4,2048]{2,1,0:T(4,128)(2,1)} %reshape.110), calls=%async_computation.1 | async-start | bytes 4194304 | tf_op jit(solution)/shard_map/all_to_all | solution.py:148
  107.5 0.0 copy-done.17
  107.5 0.1 copy.57
  107.6 3.1 %copy.59 = f32[64,4096]{1,0:T(8,128)} copy(f32[64,4096]{0,1:T(8,128)} %bitcast.50) | data formatting | bytes 2097152
  110.8 3.1 %copy.58 = f32[64,4096]{1,0:T(8,128)} copy(f32[64,4096]{0,1:T(8,128)} %bitcast.49) | data formatting | bytes 2097152
  113.9 2.1 %fusion.54 = f32[64,512]{1,0:T(8,128)S(1)} fusion(bf16[64,2048]{1,0:T(8,128)(2,1)S(1)} %fusion.24, bf16[2048,512]{1,0:T(8,128)(2,1)} %param.47), kind=kOutput, calls=%fused_computation.89 | convolution fusion | flops 134217728 | bytes 2490368 | tf_op jit(solution)/shard_map/dot_general | solution.py:72
  116.0 21.8 %all-to-all-done.1 = bf16[128,4,2048]{2,1,0:T(4,128)(2,1)} async-done(((bf16[128,4,2048]{2,1,0:T(4,128)(2,1)}), bf16[128,4,2048]{2,1,0:T(4,128)(2,1)}, u32[]{:S(2)}, u32[]{:S(2)}) %all-to-all-start.1) | async-done | bytes 2097184 | tf_op jit(solution)/shard_map/all_to_all | solution.py:148
  137.7 3.9 %reshape.111 = bf16[512,2048]{1,0:T(8,128)(2,1)} reshape(bf16[128,4,2048]{2,1,0:T(4,128)(2,1)} %all-to-all-done.1) | data formatting | bytes 4194304 | tf_op jit(solution)/shard_map/reshape | solution.py:156
  141.7 6.9 %gather_fusion.1 = bf16[384,2048]{1,0:T(8,128)(2,1)} fusion(bf16[512,2048]{1,0:T(8,128)(2,1)} %reshape.111, s32[1024]{0:T(1024)S(1)} %pad_clamp_fusion), kind=kCustom, calls=%fused_computation.1 | custom fusion | bytes 3147264 | tf_op jit(solution)/shard_map/gather | solution.py:156
  148.6 3.9 %reshape.114 = f32[64,6,2048]{2,1,0:T(8,128)} reshape(bf16[384,2048]{1,0:T(8,128)(2,1)} %gather_fusion.1) | data formatting | bytes 4718592 | tf_op jit(solution)/shard_map/convert_element_type | solution.py:158
  152.5 3.7 %multiply_reduce_fusion = f32[64,2048]{1,0:T(8,128)S(1)} fusion(f32[64,6,2048]{2,1,0:T(8,128)} %reshape.114, f32[64,6]{1,0:T(8,128)S(1)} %copy.57), kind=kLoop, calls=%fused_computation.3 | loop fusion | flops 1441792 | bytes 3671552 | tf_op jit(solution)/shard_map/reduce_sum | solution.py:160
  156.3 0.0 copy-start.15
  156.3 4.0 %multiply_reduce_fusion.1 = (f32[64]{0:T(128)S(1)}, f32[64,2048]{1,0:T(8,128)}) fusion(f32[64,2048]{1,0:T(8,128)S(1)} %multiply_reduce_fusion, bf16[512,2048]{1,0:T(8,128)(2,1)} %param.49, bf16[64,2048]{1,0:T(8,128)(2,1)S(1)} %fusion.24, bf16[2048,512]{1,0:T(8,128)(2,1)} %param.48, f32[64,512]{1,0:T(8,128)S(1)} %fusion.54), kind=kOutput, calls=%fused_computation.39 | convolution fusion | flops 269025216 | bytes 5636352 | tf_op jit(solution)/shard_map/dot_general | solution.py:75
  160.3 1.9 %fusion.25 = bf16[64,2048]{1,0:T(8,128)(2,1)} fusion(bf16[64,2048]{1,0:T(8,128)(2,1)S(1)} %get-tuple-element.13, f32[64,2048]{1,0:T(8,128)} %get-tuple-element.21, f32[2048]{0:T(1024)S(1)} %copy-done.15, f32[64]{0:T(128)S(1)} %add_rsqrt_fusion), kind=kLoop, calls=%fused_computation.38 | loop fusion | flops 655360 | bytes 1057024 | tf_op jit(solution)/shard_map/convert_element_type | solution.py:163
  (22 shorter events, 0.1 us)
Async XLA Ops:
  0.6 90.8 %copy-start = (bf16[1,512,2048]{2,1,0:T(8,128)(2,1)S(1)}, bf16[1,512,2048]{2,1,0:T(8,128)(2,1)}, u32[]{:S(2)}) copy-start(bf16[1,512,2048]{2,1,0:T(8,128)(2,1)} %param.46) | copy-start | bytes 6291460
  7.2 3.2 %copy-start.11 = (f32[64,64]{1,0:T(8,128)S(1)}, f32[64,64]{1,0:T(8,128)}, u32[]{:S(2)}) copy-start(f32[64,64]{1,0:T(8,128)} %param.30) | copy-start | bytes 49156
  7.2 3.2 %copy-start.12 = (f32[64,64]{1,0:T(8,128)S(1)}, f32[64,64]{1,0:T(8,128)}, u32[]{:S(2)}) copy-start(f32[64,64]{1,0:T(8,128)} %param.29) | copy-start | bytes 49156
  7.2 3.4 %copy-start.5 = (bf16[64,64,16]{1,2,0:T(8,128)(2,1)S(1)}, bf16[64,64,16]{1,2,0:T(8,128)(2,1)}, u32[]{:S(2)}) copy-start(bf16[64,64,16]{1,2,0:T(8,128)(2,1)} %param.32) | copy-start | bytes 393220
  7.2 3.4 %copy-start.6 = (bf16[64,64,16]{1,2,0:T(8,128)(2,1)S(1)}, bf16[64,64,16]{1,2,0:T(8,128)(2,1)}, u32[]{:S(2)}) copy-start(bf16[64,64,16]{1,2,0:T(8,128)(2,1)} %param.33) | copy-start | bytes 393220
  10.6 6.0 %copy-start.1 = (f32[64,4096]{0,1:T(8,128)S(1)}, f32[64,4096]{0,1:T(8,128)}, u32[]{:S(2)}) copy-start(f32[64,4096]{0,1:T(8,128)} %copy.49) | copy-start | bytes 3145732
  10.6 6.0 %copy-start.2 = (f32[64,4096]{0,1:T(8,128)S(1)}, f32[64,4096]{0,1:T(8,128)}, u32[]{:S(2)}) copy-start(f32[64,4096]{0,1:T(8,128)} %copy.50) | copy-start | bytes 3145732
  16.7 7.7 %copy-start.9 = (bf16[64,16,64]{2,1,0:T(8,128)(2,1)S(1)}, bf16[64,16,64]{2,1,0:T(8,128)(2,1)}, u32[]{:S(2)}) copy-start(bf16[64,16,64]{2,1,0:T(8,128)(2,1)} %param.34) | copy-start | bytes 393220
  20.7 6.5 %copy-start.10 = (bf16[64,16,64]{2,1,0:T(8,128)(2,1)S(1)}, bf16[64,16,64]{2,1,0:T(8,128)(2,1)}, u32[]{:S(2)}) copy-start(bf16[64,16,64]{2,1,0:T(8,128)(2,1)} %param.35) | copy-start | bytes 393220
  24.3 2.9 %copy-start.3 = (f32[64,64,64]{0,2,1:T(8,128)S(1)}, f32[64,64,64]{0,2,1:T(8,128)}, u32[]{:S(2)}) copy-start(f32[64,64,64]{0,2,1:T(8,128)} %bitcast_add_fusion) | copy-start | bytes 3145732
  27.2 1.3 copy-start.7
  27.2 1.3 copy-start.16
  28.7 3.5 %copy-start.4 = (bf16[1024,2048]{1,0:T(8,128)(2,1)S(1)}, bf16[1024,2048]{1,0:T(8,128)(2,1)}, u32[]{:S(2)}) copy-start(bf16[1024,2048]{1,0:T(8,128)(2,1)} %param.37) | copy-start | bytes 12582916
  32.1 1.0 copy-start.8
  32.1 1.0 copy-start.13
  32.1 1.3 copy-start.14
  101.9 5.6 %copy-start.17 = (f32[64,6]{0,1:T(8,128)S(1)}, f32[64,6]{0,1:T(8,128)}, u32[]{:S(2)}) copy-start(f32[64,6]{0,1:T(8,128)} %param.43) | copy-start | bytes 4612
  101.9 35.8 %all-to-all-start.1 = ((bf16[128,4,2048]{2,1,0:T(4,128)(2,1)}), bf16[128,4,2048]{2,1,0:T(4,128)(2,1)}, u32[]{:S(2)}, u32[]{:S(2)}) async-start(bf16[128,4,2048]{2,1,0:T(4,128)(2,1)} %reshape.110), calls=%async_computation.1 | async-start | bytes 4194304 | tf_op jit(solution)/shard_map/all_to_all | solution.py:148
  156.3 4.1 %copy-start.15 = (f32[2048]{0:T(1024)S(1)}, f32[2048]{0:T(1024)}, u32[]{:S(2)}) copy-start(f32[2048]{0:T(1024)} %param.41) | copy-start | bytes 24580
where the time goes:
time: 163 us; the launch traced here: 162 us
  local copies, waits for them, and re-layouts  49.4 us (30%)
  blocking collectives  42.1 us (26%)
  matrix products  35 us (21%)
  waiting for transfers between devices  21.8 us (13%)
  other arithmetic  7.54 us (5%)
  starting transfers between devices  5.59 us (3%)
    all_to_all x1, blocking collectives, serve_rows(): lax.all_to_all(outgoing, 'ep', split_axis=0, concat_axis=0, tiled=True)  42.1 us
    all_to_all x1, waiting for transfers between devices, serve_rows(): lax.all_to_all(produced.reshape(source_count, item_count, hidden_width),...  21.8 us
    unnamed x43, local copies, waits for them, and re-layouts  14.9 us
    dot_general x2, matrix products, expert_rows(): return jnp.dot(hidden, w_down, preferred_element_type=jnp.float32)  10.3 us
    gather x1, local copies, waits for them, and re-layouts, serve_rows(): returned.reshape(-1, hidden_width)[slot_index]  6.93 us
    dot_general x2, matrix products, expert_rows(): gate_part = jnp.dot(row_block, w_gate, preferred_element_type=jnp.float32)  6.5 us
    dot_general x1, matrix products, state_step(): jnp.einsum('tgc,gpc->tgp', feed_rows, bbar_im, precision=lax.Precision.HI...  5.99 us
    all_to_all x1, starting transfers between devices, serve_rows(): lax.all_to_all(produced.reshape(source_count, item_count, hidden_width),...  5.59 us
  transfers between devices with their start and end apart: 1, of which 1 were waited for; matrix products, arithmetic and copies ran while one was open for 5% of the time, Pallas kernels for 0%

commit v1 on v0

v1 whole, which is shorter than its diff:
```python
import functools

import jax
import jax.numpy as jnp
from jax import lax
from jax.experimental import pallas as pl
from jax.experimental.pallas import tpu as pltpu
from jax.sharding import PartitionSpec as P

MESH = pl.DeviceIdType.MESH
F32 = jnp.float32
BF16 = jnp.bfloat16
EPS = 1e-06
N_DEV = 128
CAP = 4
SLOTS = N_DEV * CAP
STRIDE = 43
STRIDE_INV = pow(STRIDE, -1, N_DEV)
GROUPS = 4
GROUP_DEV = N_DEV // GROUPS
GROUP_ROWS = SLOTS // GROUPS
NT = (((1,), (1,)), ((), ()))
TN = (((0,), (0,)), ((), ()))


def split_hi_lo(value):
    hi = value.astype(BF16)
    lo = (value - hi.astype(F32)).astype(BF16)
    return hi, lo


SSM_STEPS = 4
BLOCKS_PER_STEP = 8 // SSM_STEPS


def state_kernel(
    feed_ref,
    re_ref,
    im_ref,
    decay_ref,
    freq_ref,
    log_step_ref,
    in_re_ref,
    in_im_ref,
    out_re_ref,
    out_im_ref,
    skip_ref,
    next_re_ref,
    next_im_ref,
    act_ref,
):
    step = pl.program_id(0)
    rows = 8 * BLOCKS_PER_STEP
    group = lax.broadcasted_iota(jnp.int32, (rows, 64), 0) + step * rows
    lane = lax.broadcasted_iota(jnp.int32, (rows, 64), 1)
    column = jnp.sum(
        jnp.where(group == lane, jnp.broadcast_to(log_step_ref[...], (rows, 64)), 0.0),
        axis=1,
        keepdims=True,
    )
    step_size = jnp.exp(column)
    decay = decay_ref[...]
    freq = freq_ref[...]
    magnitude = jnp.exp(-decay * step_size)
    phase = freq * step_size
    abar_re = magnitude * jnp.cos(phase)
    abar_im = magnitude * jnp.sin(phase)
    denominator = decay * decay + freq * freq
    numer_re = abar_re - 1.0
    coef_re = (abar_im * freq - numer_re * decay) / denominator
    coef_im = (-abar_im * decay - numer_re * freq) / denominator

    def twice(v):
        return jnp.concatenate([v, v], axis=1)

    abar_re, abar_im, coef_re, coef_im = map(
        twice, (abar_re, abar_im, coef_re, coef_im)
    )
    row_group = lax.broadcasted_iota(jnp.int32, (128, 128), 0) // 16
    lane_half = lax.broadcasted_iota(jnp.int32, (128, 128), 1) // 64
    low_half = lax.broadcasted_iota(jnp.int32, (1, 128), 1) < 64
    for b in range(BLOCKS_PER_STEP):
        bb_re, bb_im = [], []
        for g in range(8):
            r = b * 8 + g
            own = slice(r * 16, r * 16 + 16)
            b_re = twice(in_re_ref[own, :].astype(F32))
            b_im = twice(in_im_ref[own, :].astype(F32))
            c_re, c_im = coef_re[r : r + 1, :], coef_im[r : r + 1, :]
            bb_re.append(c_re * b_re - c_im * b_im)
            bb_im.append(c_re * b_im + c_im * b_re)
        bb_re = jnp.concatenate(bb_re, axis=0)
        bb_im = jnp.concatenate(bb_im, axis=0)
        rows_here = slice(b * 128, b * 128 + 128)
        o_re = twice(out_re_ref[rows_here, :].astype(F32))
        o_im = twice(-out_im_ref[rows_here, :].astype(F32))
        parts_re_hi, parts_re_lo = split_hi_lo(bb_re)
        parts_im_hi, parts_im_lo = split_hi_lo(bb_im)
        feed = feed_ref[:, b * 128 : b * 128 + 128]
        feed_twice = jnp.concatenate([feed, feed], axis=1)
        readout = jnp.zeros((64, 128), F32)
        for q in range(4):
            mask = row_group == 2 * q + lane_half
            zero = jnp.zeros((128, 128), BF16)

            def block(hi, lo):
                return jnp.concatenate(
                    [jnp.where(mask, hi, zero), jnp.where(mask, lo, zero)], axis=0
                )

            f_re = jnp.dot(
                feed_twice, block(parts_re_hi, parts_re_lo), preferred_element_type=F32
            )
            f_im = jnp.dot(
                feed_twice, block(parts_im_hi, parts_im_lo), preferred_element_type=F32
            )
            r0 = b * 8 + 2 * q
            a_re = jnp.where(
                low_half, abar_re[r0 : r0 + 1, :], abar_re[r0 + 1 : r0 + 2, :]
            )
            a_im = jnp.where(
                low_half, abar_im[r0 : r0 + 1, :], abar_im[r0 + 1 : r0 + 2, :]
            )
            lanes = slice(b * 512 + q * 128, b * 512 + q * 128 + 128)
            old_re, old_im = re_ref[:, lanes], im_ref[:, lanes]
            new_re = a_re * old_re - a_im * old_im + f_re
            new_im = a_re * old_im + a_im * old_re + f_im
            next_re_ref[:, lanes] = new_re
            next_im_ref[:, lanes] = new_im
            re_hi, re_lo = split_hi_lo(new_re)
            im_hi, im_lo = split_hi_lo(new_im)
            w = jnp.concatenate(
                [
                    jnp.where(mask, o_re, 0.0).astype(BF16),
                    jnp.where(mask, o_im, 0.0).astype(BF16),
                ],
                axis=1,
            )
            left = jnp.concatenate(
                [
                    jnp.concatenate([re_hi, im_hi], axis=1),
                    jnp.concatenate([re_lo, im_lo], axis=1),
                ],
                axis=0,
            )
            both = lax.dot_general(left, w, NT, preferred_element_type=F32)
            readout = readout + (both[:64] + both[64:])
        here = slice(b * 128, b * 128 + 128)
        mixed = readout + skip_ref[:, here] * feed.astype(F32)
        act_ref[:, here] = jax.nn.gelu(mixed).astype(BF16)


def state_step(
    branch_in,
    state_real,
    state_imag,
    decay_rate,
    frequency,
    log_step,
    input_real,
    input_imag,
    output_matrix_real,
    output_matrix_imaginary,
    skip_gain,
):
    in_re = jnp.transpose(input_real, (0, 2, 1)).reshape(1024, 64)
    in_im = jnp.transpose(input_imag, (0, 2, 1)).reshape(1024, 64)
    out_re = output_matrix_real.reshape(1024, 64)
    out_im = output_matrix_imaginary.reshape(1024, 64)
    n = SSM_STEPS
    wide = pl.BlockSpec((64, 4096 // n), lambda i: (0, i))
    narrow = pl.BlockSpec((64, 1024 // n), lambda i: (0, i))
    per_group = pl.BlockSpec((64 // n, 64), lambda i: (i, 0))
    per_channel = pl.BlockSpec((1024 // n, 64), lambda i: (i, 0))
    return pl.pallas_call(
        state_kernel,
        grid=(n,),
        out_shape=(
            jax.ShapeDtypeStruct((64, 4096), F32),
            jax.ShapeDtypeStruct((64, 4096), F32),
            jax.ShapeDtypeStruct((64, 1024), BF16),
        ),
        in_specs=[
            narrow,
            wide,
            wide,
            per_group,
            per_group,
            pl.BlockSpec((1, 64), lambda i: (0, 0)),
            per_channel,
            per_channel,
            per_channel,
            per_channel,
            pl.BlockSpec((1, 1024 // n), lambda i: (0, i)),
        ],
        out_specs=(wide, wide, narrow),
        compiler_params=pltpu.CompilerParams(
            dimension_semantics=("arbitrary",), vmem_limit_bytes=20 * 2**20
        ),
        name="state_step",
    )(
        branch_in,
        state_real,
        state_imag,
        decay_rate,
        frequency,
        log_step.reshape(1, 64),
        in_re,
        in_im,
        out_re,
        out_im,
        skip_gain.reshape(1, 1024),
    )


def torus_add(me, off):
    core = lax.rem(me + off, 2)
    x = lax.rem(me // 2 + off // 2, 4)
    y = lax.rem(me // 8 + off // 8, 4)
    z = lax.rem(me // 32 + off // 32, 4)
    return ((z * 4 + y) * 4 + x) * 2 + core


def torus_sub(me, off):
    core = lax.rem(me + off, 2)
    x = lax.rem(me // 2 + 4 - lax.rem(off // 2, 4), 4)
    y = lax.rem(me // 8 + 4 - lax.rem(off // 8, 4), 4)
    z = lax.rem(me // 32 + 4 - off // 32, 4)
    return ((z * 4 + y) * 4 + x) * 2 + core


def offset_of(position):
    return lax.rem(position * STRIDE, N_DEV)


def inv_rms(v):
    return lax.rsqrt(jnp.mean(v * v, axis=-1, keepdims=True) + EPS)


def expert_kernel(
    act_ref,
    resid_ref,
    mix_gain_ref,
    in_gain_ref,
    out_gain_ref,
    routes_ref,
    weights_ref,
    glu_value_hbm,
    glu_gate_hbm,
    e_gate_hbm,
    e_up_hbm,
    e_down_hbm,
    s_gate_hbm,
    s_up_hbm,
    s_down_hbm,
    out_ref,
    glu_value,
    glu_gate,
    e_gate,
    e_up,
    e_down,
    s_gate,
    s_up,
    s_down,
    branch,
    resid_mid,
    normed,
    pick,
    weight_hi,
    weight_lo,
    total,
    outgoing,
    received,
    produced,
    returned,
    load_sem,
    send_sem,
    recv_sem,
    back_send_sem,
    back_recv_sem,
):
    me = lax.axis_index("ep")
    barrier = pltpu.get_barrier_semaphore()

    def greet(i, carry):
        pl.semaphore_signal(
            barrier, inc=1, device_id=(lax.rem(me + i, N_DEV),), device_id_type=MESH
        )
        return carry

    lax.fori_loop(1, N_DEV, greet, 0)

    loads = []

    def load(src, dst):
        copy = pltpu.make_async_copy(src, dst, load_sem.at[len(loads)])
        copy.start()
        loads.append(copy)
        return copy

    glu_loads = []
    for n in range(4):
        cols = pl.ds(n * 512, 512)
        glu_loads.append(
            (
                load(glu_value_hbm.at[:, cols], glu_value.at[:, cols]),
                load(glu_gate_hbm.at[:, cols], glu_gate.at[:, cols]),
            )
        )
    s_loads = [load(s_gate_hbm, s_gate), load(s_up_hbm, s_up), load(s_down_hbm, s_down)]
    e_loads = [load(e_gate_hbm, e_gate), load(e_up_hbm, e_up), load(e_down_hbm, e_down)]

    routes = routes_ref[...]
    rel = (
        jnp.bitwise_and(routes + me, 1)
        + jnp.bitwise_and((routes >> 1) + 4 - lax.rem(me // 2, 4), 3) * 2
        + jnp.bitwise_and((routes >> 3) + 4 - lax.rem(me // 8, 4), 3) * 8
        + jnp.bitwise_and((routes >> 5) + 4 - me // 32, 3) * 32
    )
    position = jnp.bitwise_and(rel * STRIDE_INV, N_DEV - 1)
    row = lax.broadcasted_iota(jnp.int32, (SLOTS, 64), 0)
    row_pos = row >> 2
    row_rank = jnp.bitwise_and(row, 3).astype(F32)
    named = jnp.zeros((SLOTS, 64), F32)
    weight = jnp.zeros((SLOTS, 64), F32)
    for k in range(6):
        hit = row_pos == position[k : k + 1, :]
        named = jnp.where(hit, 1.0, named)
        weight = jnp.where(hit, weights_ref[k : k + 1, :], weight)
    earlier = (
        lax.broadcasted_iota(jnp.int32, (64, 64), 0)
        < lax.broadcasted_iota(jnp.int32, (64, 64), 1)
    ).astype(BF16)
    rank = jnp.dot(named.astype(BF16), earlier, preferred_element_type=F32)
    chosen = rank == row_rank
    pick[...] = jnp.where(chosen, named, 0.0).astype(BF16)
    hi, lo = split_hi_lo(jnp.where(chosen, weight, 0.0))
    weight_hi[...] = hi
    weight_lo[...] = lo

    act = act_ref[...]
    square = jnp.zeros((64, 1), F32)
    for n in range(4):
        cols = slice(n * 512, n * 512 + 512)
        for copy in glu_loads[n]:
            copy.wait()
        value_part = jnp.dot(act, glu_value[:, cols], preferred_element_type=F32)
        gate_part = jnp.dot(act, glu_gate[:, cols], preferred_element_type=F32)
        part = value_part * jax.nn.sigmoid(gate_part)
        branch[:, cols] = part
        square = square + jnp.sum(part * part, axis=-1, keepdims=True)
    scale = lax.rsqrt(square * (1.0 / 2048) + EPS)
    mid = (
        resid_ref[...].astype(F32) + branch[...] * scale * mix_gain_ref[...]
    ).astype(BF16)
    resid_mid[...] = mid
    mid = mid.astype(F32)
    normed[...] = (mid * inv_rms(mid) * in_gain_ref[...]).astype(BF16)

    for n in range(4):
        cols = slice(n * 512, n * 512 + 512)
        outgoing[:, cols] = jnp.dot(
            pick[...], normed[:, cols], preferred_element_type=F32
        ).astype(BF16)
    pl.semaphore_wait(barrier, N_DEV - 1)

    def slot(i):
        return pl.ds(pl.multiple_of(i * CAP, CAP), CAP)

    pltpu.make_async_copy(
        outgoing.at[slot(0), :], received.at[slot(0), :], recv_sem.at[0]
    ).start()

    def send(i, carry):
        pltpu.make_async_remote_copy(
            src_ref=outgoing.at[slot(i), :],
            dst_ref=received.at[slot(i), :],
            send_sem=send_sem,
            recv_sem=recv_sem.at[i // GROUP_DEV],
            device_id=(torus_add(me, offset_of(i)),),
            device_id_type=MESH,
        ).start()
        return carry

    lax.fori_loop(1, N_DEV, send, 0)

    for copy in s_loads:
        copy.wait()
    x = normed[...]
    g = jnp.dot(x, s_gate[...], preferred_element_type=F32)
    u = jnp.dot(x, s_up[...], preferred_element_type=F32)
    hidden = (jax.nn.silu(g) * u).astype(BF16)
    for n in range(4):
        cols = slice(n * 512, n * 512 + 512)
        total[:, cols] = jnp.dot(hidden, s_down[:, cols], preferred_element_type=F32)
    for copy in e_loads:
        copy.wait()

    def wait_group(buffer, sem, first, rows):
        part = buffer.at[pl.ds(first, rows), :]
        pltpu.make_async_copy(part, part, sem).wait()

    def back(i, carry):
        pltpu.make_async_remote_copy(
            src_ref=produced.at[slot(i), :],
            dst_ref=returned.at[slot(i), :],
            send_sem=back_send_sem,
            recv_sem=back_recv_sem.at[i // GROUP_DEV],
            device_id=(torus_sub(me, offset_of(i)),),
            device_id_type=MESH,
        ).start()
        return carry

    def run_group(first):
        rows = pl.ds(first, GROUP_ROWS)
        x = received[rows, :]
        g = jnp.dot(x, e_gate[...], preferred_element_type=F32)
        u = jnp.dot(x, e_up[...], preferred_element_type=F32)
        hidden = (jax.nn.silu(g) * u).astype(BF16)
        for n in range(4):
            cols = slice(n * 512, n * 512 + 512)
            produced[rows, cols] = jnp.dot(
                hidden, e_down[:, cols], preferred_element_type=F32
            ).astype(BF16)

    wait_group(received, recv_sem.at[0], 0, GROUP_ROWS)
    run_group(0)
    pltpu.make_async_copy(
        produced.at[slot(0), :], returned.at[slot(0), :], back_recv_sem.at[0]
    ).start()
    lax.fori_loop(1, GROUP_DEV, back, 0)

    def one_group(g, carry):
        first = pl.multiple_of(g * GROUP_ROWS, GROUP_ROWS)
        wait_group(received, recv_sem.at[g], first, GROUP_ROWS)
        run_group(first)
        lax.fori_loop(g * GROUP_DEV, (g + 1) * GROUP_DEV, back, 0)
        return carry

    lax.fori_loop(1, GROUPS, one_group, 0)

    def add_group(first):
        rows = pl.ds(first, GROUP_ROWS)
        left = jnp.concatenate([weight_hi[rows, :], weight_lo[rows, :]], axis=1)
        for n in range(4):
            cols = slice(n * 512, n * 512 + 512)
            both = lax.dot_general(
                left, returned[rows, cols], TN, preferred_element_type=F32
            )
            total[:, cols] += both[:64] + both[64:]

    wait_group(returned, back_recv_sem.at[0], 0, GROUP_ROWS)
    add_group(0)

    def add_one(g, carry):
        first = pl.multiple_of(g * GROUP_ROWS, GROUP_ROWS)
        wait_group(returned, back_recv_sem.at[g], first, GROUP_ROWS)
        add_group(first)
        return carry

    lax.fori_loop(1, GROUPS, add_one, 0)

    combined = total[...]
    out_ref[...] = (
        resid_mid[...].astype(F32)
        + combined * inv_rms(combined) * out_gain_ref[...]
    ).astype(BF16)
    wait_group(s_gate, send_sem, 0, (SLOTS - CAP) * 4)
    wait_group(s_gate, back_send_sem, 0, (SLOTS - CAP) * 4)


def experts(
    activated,
    residual,
    mix_gain,
    moe_in_gain,
    moe_out_gain,
    routes,
    route_weights,
    weights,
):
    vmem = pl.BlockSpec(memory_space=pltpu.VMEM)
    hbm = pl.BlockSpec(memory_space=pl.ANY)
    return pl.pallas_call(
        expert_kernel,
        out_shape=jax.ShapeDtypeStruct((64, 2048), BF16),
        in_specs=[vmem] * 7 + [hbm] * 8,
        out_specs=vmem,
        scratch_shapes=[
            pltpu.VMEM((1024, 2048), BF16),
            pltpu.VMEM((1024, 2048), BF16),
            pltpu.VMEM((2048, 512), BF16),
            pltpu.VMEM((2048, 512), BF16),
            pltpu.VMEM((512, 2048), BF16),
            pltpu.VMEM((2048, 512), BF16),
            pltpu.VMEM((2048, 512), BF16),
            pltpu.VMEM((512, 2048), BF16),
            pltpu.VMEM((64, 2048), F32),
            pltpu.VMEM((64, 2048), BF16),
            pltpu.VMEM((64, 2048), BF16),
            pltpu.VMEM((SLOTS, 64), BF16),
            pltpu.VMEM((SLOTS, 64), BF16),
            pltpu.VMEM((SLOTS, 64), BF16),
            pltpu.VMEM((64, 2048), F32),
            pltpu.VMEM((SLOTS, 2048), BF16),
            pltpu.VMEM((SLOTS, 2048), BF16),
            pltpu.VMEM((SLOTS, 2048), BF16),
            pltpu.VMEM((SLOTS, 2048), BF16),
            pltpu.SemaphoreType.DMA((14,)),
            pltpu.SemaphoreType.DMA,
            pltpu.SemaphoreType.DMA((GROUPS,)),
            pltpu.SemaphoreType.DMA,
            pltpu.SemaphoreType.DMA((GROUPS,)),
        ],
        compiler_params=pltpu.CompilerParams(
            collective_id=0, has_side_effects=True, vmem_limit_bytes=52 * 2**20
        ),
        name="experts",
    )(
        activated,
        residual,
        mix_gain.reshape(1, 2048),
        moe_in_gain.reshape(1, 2048),
        moe_out_gain.reshape(1, 2048),
        jnp.transpose(routes),
        jnp.transpose(route_weights),
        *weights,
    )


def per_device(
    residual,
    branch_in,
    state_real,
    state_imag,
    decay_rate,
    frequency,
    log_step,
    input_real,
    input_imag,
    output_matrix_real,
    output_matrix_imaginary,
    skip_gain,
    glu_value,
    glu_gate,
    mix_gain,
    moe_in_gain,
    moe_out_gain,
    routes,
    route_weights,
    expert_gate,
    expert_up,
    expert_down,
    shared_gate,
    shared_up,
    shared_down,
):
    next_real, next_imag, activated = state_step(
        branch_in,
        state_real,
        state_imag,
        decay_rate,
        frequency,
        log_step,
        input_real,
        input_imag,
        output_matrix_real,
        output_matrix_imaginary,
        skip_gain,
    )
    layer_out = experts(
        activated,
        residual,
        mix_gain,
        moe_in_gain,
        moe_out_gain,
        routes,
        route_weights,
        (
            glu_value,
            glu_gate,
            expert_gate.reshape(2048, 512),
            expert_up.reshape(2048, 512),
            expert_down.reshape(512, 2048),
            shared_gate,
            shared_up,
            shared_down,
        ),
    )
    return layer_out, next_real, next_imag


def solution(mesh):
    return jax.shard_map(
        per_device,
        mesh=mesh,
        in_specs=(
            P("ep", None),
            P("ep", None),
            P("ep", None),
            P("ep", None),
            P(),
            P(),
            P(),
            P(),
            P(),
            P(),
            P(),
            P(),
            P(),
            P(),
            P(),
            P(),
            P(),
            P("ep", None),
            P("ep", None),
            P("ep", None, None),
            P("ep", None, None),
            P("ep", None, None),
            P(),
            P(),
            P(),
        ),
        out_specs=(P("ep", None), P("ep", None), P("ep", None)),
        check_vma=False,
    )
```

time: 163 us -> 82.9 us (0.51)
  Pallas kernels: 0 us -> 70.6 us
  blocking collectives: 42.1 us -> 0 us
  local copies, waits for them, and re-layouts: 49.4 us -> 10.7 us
  matrix products: 35 us -> 0 us
  waiting for transfers between devices: 21.8 us -> 0 us
  other arithmetic: 7.54 us -> 0 us
  starting transfers between devices: 5.59 us -> 0 us
    pallas_call x0 -> x2, Pallas kernels: none -> 70.6 us  [the longest x1 66.2 us: experts(): pl.pallas_call(expert_kernel, out_shape=jax.ShapeDtypeStruct((64, 2048),...]
    all_to_all x1 -> x0, blocking collectives: 42.1 us -> none  [serve_rows(): lax.all_to_all(outgoing, 'ep', split_axis=0, concat_axis=0, tiled=True)]
    dot_general x10 -> x0, matrix products: 35 us -> none  [the longest x2 10.3 us: expert_rows(): return jnp.dot(hidden, w_down, preferred_element_type=jnp.float32)]
    all_to_all x1 -> x0, waiting for transfers between devices: 21.8 us -> none  [serve_rows(): lax.all_to_all(produced.reshape(source_count, item_count, hidden_width),...]
    reshape x5 -> x0, local copies, waits for them, and re-layouts: 16.4 us -> none  [the longest x1 4.15 us: serve_rows(): produced.reshape(source_count, item_count, hidden_width)]
    gather x2 -> x0, local copies, waits for them, and re-layouts: 10.2 us -> none  [the longest x1 6.93 us: serve_rows(): returned.reshape(-1, hidden_width)[slot_index]]
    all_to_all x1 -> x0, starting transfers between devices: 5.59 us -> none  [serve_rows(): lax.all_to_all(produced.reshape(source_count, item_count, hidden_width),...]
    reduce_sum x3 -> x0, other arithmetic: 4.26 us -> none  [the longest x1 3.74 us: serve_rows(): routed = jnp.sum(per_assign * route_weights[..., None], axis=1)]
  transfers between devices with their start and end apart: 1 -> 0, of which waited for: 1 -> 0; matrix products, arithmetic and copies ran while one was open for 5% -> 0% of each run, Pallas kernels for 0% -> 0%
where the time goes in v1:
time: 82.9 us; the launch traced here: 82.1 us
  Pallas kernels  70.6 us (85%)
  local copies, waits for them, and re-layouts  10.7 us (13%)
    pallas_call x1, Pallas kernels, experts(): pl.pallas_call(expert_kernel, out_shape=jax.ShapeDtypeStruct((64, 2048),...  66.2 us
    unnamed x35, local copies, waits for them, and re-layouts  10.7 us
    pallas_call x1, Pallas kernels, state_step(): pl.pallas_call(state_kernel, grid=(n,), out_shape=(jax.ShapeDtypeStruct((...  4.41 us

profile of v1, /device:TPU:1, one launch (start us, length us, event | category | flops | bytes accessed | tf_op | source)
XLA Modules:
  0.0 82.1 jit_solution(17919870278609509461)
XLA Ops:
  0.6 0.0 copy-start.12
  0.6 0.0 copy-start.11
  0.7 0.0 copy-start.10
  0.7 0.0 copy-start
  0.7 1.2 %copy-done = f32[64,4096]{1,0:T(8,128)S(1)} copy-done((f32[64,4096]{1,0:T(8,128)S(1)}, f32[64,4096]{1,0:T(8,128)}, u32[]{:S(2)}) %copy-start) | copy-done | bytes 1048600
  1.9 0.0 copy-start.1
  1.9 1.2 %copy-done.1 = f32[64,4096]{1,0:T(8,128)S(1)} copy-done((f32[64,4096]{1,0:T(8,128)S(1)}, f32[64,4096]{1,0:T(8,128)}, u32[]{:S(2)}) %copy-start.1) | copy-done | bytes 1048600
  3.1 0.0 copy-start.3
  3.1 0.9 %copy-done.3 = bf16[64,64,16]{1,2,0:T(8,128)(2,1)S(1)} copy-done((bf16[64,64,16]{1,2,0:T(8,128)(2,1)S(1)}, bf16[64,64,16]{1,2,0:T(8,128)(2,1)}, u32[]{:S(2)}) %copy-start.3) | copy-done | bytes 131096
  4.1 0.0 copy-start.4
  4.1 0.9 %copy-done.4 = bf16[64,64,16]{1,2,0:T(8,128)(2,1)S(1)} copy-done((bf16[64,64,16]{1,2,0:T(8,128)(2,1)S(1)}, bf16[64,64,16]{1,2,0:T(8,128)(2,1)}, u32[]{:S(2)}) %copy-start.4) | copy-done | bytes 131096
  5.0 0.0 copy-start.5
  5.0 0.9 %copy-done.5 = bf16[64,16,64]{2,1,0:T(8,128)(2,1)S(1)} copy-done((bf16[64,16,64]{2,1,0:T(8,128)(2,1)S(1)}, bf16[64,16,64]{2,1,0:T(8,128)(2,1)}, u32[]{:S(2)}) %copy-start.5) | copy-done | bytes 131096
  6.0 0.0 copy-start.6
  6.0 0.9 %copy-done.6 = bf16[64,16,64]{2,1,0:T(8,128)(2,1)S(1)} copy-done((bf16[64,16,64]{2,1,0:T(8,128)(2,1)S(1)}, bf16[64,16,64]{2,1,0:T(8,128)(2,1)}, u32[]{:S(2)}) %copy-start.6) | copy-done | bytes 131096
  6.9 0.0 copy-start.7
  6.9 0.9 %copy-done.7 = bf16[64,1024]{1,0:T(8,128)(2,1)S(1)} copy-done((bf16[64,1024]{1,0:T(8,128)(2,1)S(1)}, bf16[64,1024]{1,0:T(8,128)(2,1)}, u32[]{:S(2)}) %copy-start.7) | copy-done | bytes 131096
  7.8 0.0 copy-start.8
  7.8 0.8 copy-done.8
  8.6 0.0 copy-start.9
  8.6 0.8 copy-done.9
  9.4 0.0 copy-start.13
  9.4 0.7 copy-done.13
  10.0 0.0 copy-start.16
  10.0 0.7 copy-done.16
  10.7 0.0 copy-start.2
  10.7 0.0 copy-start.14
  10.7 0.0 copy-start.15
  10.7 4.4 %state_step.1 = (f32[64,4096]{1,0:T(8,128)}, f32[64,4096]{1,0:T(8,128)}, bf16[64,1024]{1,0:T(8,128)(2,1)S(1)}) custom-call(bf16[64,1024]{1,0:T(8,128)(2,1)S(1)} %copy-done.7, f32[64,4096]{1,0:T(8,128)S(1)} %copy-done, f32[64,4096]{1,0:T(8,128)S(1)} %copy-done.1, f32[64,64]{1,0:T(8,128)S(1)} %copy-done.8, f32[64,64]{1,0:T(8,128)S(1)} %copy-done.9, ...), custom_call_target="tpu_custom_call" | custom-call | tf_op jit(solution)/shard_map/state_step/pallas_call | solution.py:175
  15.1 0.0 copy-done.12
  15.1 0.0 copy-done.11
  15.1 0.0 copy-done.10
  15.1 0.0 copy-done.2
  15.1 0.0 copy-done.14
  15.1 0.0 copy-done.15
  15.2 66.2 %experts.1 = bf16[64,2048]{1,0:T(8,128)(2,1)S(1)} custom-call(bf16[64,1024]{1,0:T(8,128)(2,1)S(1)} %get-tuple-element.6.act_ref, bf16[64,2048]{1,0:T(8,128)(2,1)S(1)} %copy-done.2, f32[1,2048]{1,0:T(1,128)S(1)} %bitcast.22, f32[1,2048]{1,0:T(1,128)S(1)} %bitcast.23, f32[1,2048]{1,0:T(1,128)S(1)} %bitcast.24, s32[6,64]{1,0:T(8,128)S(1)} %bitcast.26, ...), custom_call_target="tpu_custom_call" | custom-call | tf_op jit(solution)/shard_map/experts/pallas_call | solution.py:484
  81.4 0.7 copy.29
Async XLA Ops:
  0.6 14.5 %copy-start.12 = (f32[2048]{0:T(1024)S(1)}, f32[2048]{0:T(1024)}, u32[]{:S(2)}) copy-start(f32[2048]{0:T(1024)} %param.41) | copy-start | bytes 24580
  0.6 14.5 %copy-start.11 = (f32[2048]{0:T(1024)S(1)}, f32[2048]{0:T(1024)}, u32[]{:S(2)}) copy-start(f32[2048]{0:T(1024)} %param.40) | copy-start | bytes 24580
  0.7 14.5 %copy-start.10 = (f32[2048]{0:T(1024)S(1)}, f32[2048]{0:T(1024)}, u32[]{:S(2)}) copy-start(f32[2048]{0:T(1024)} %param.39) | copy-start | bytes 24580
  0.7 1.2 %copy-start = (f32[64,4096]{1,0:T(8,128)S(1)}, f32[64,4096]{1,0:T(8,128)}, u32[]{:S(2)}) copy-start(f32[64,4096]{1,0:T(8,128)} %re_ref.1) | copy-start | bytes 3145732
  1.9 1.2 %copy-start.1 = (f32[64,4096]{1,0:T(8,128)S(1)}, f32[64,4096]{1,0:T(8,128)}, u32[]{:S(2)}) copy-start(f32[64,4096]{1,0:T(8,128)} %im_ref.1) | copy-start | bytes 3145732
  3.1 0.9 %copy-start.3 = (bf16[64,64,16]{1,2,0:T(8,128)(2,1)S(1)}, bf16[64,64,16]{1,2,0:T(8,128)(2,1)}, u32[]{:S(2)}) copy-start(bf16[64,64,16]{1,2,0:T(8,128)(2,1)} %param.32) | copy-start | bytes 393220
  4.1 0.9 %copy-start.4 = (bf16[64,64,16]{1,2,0:T(8,128)(2,1)S(1)}, bf16[64,64,16]{1,2,0:T(8,128)(2,1)}, u32[]{:S(2)}) copy-start(bf16[64,64,16]{1,2,0:T(8,128)(2,1)} %param.33) | copy-start | bytes 393220
  5.0 0.9 %copy-start.5 = (bf16[64,16,64]{2,1,0:T(8,128)(2,1)S(1)}, bf16[64,16,64]{2,1,0:T(8,128)(2,1)}, u32[]{:S(2)}) copy-start(bf16[64,16,64]{2,1,0:T(8,128)(2,1)} %param.34) | copy-start | bytes 393220
  6.0 0.9 %copy-start.6 = (bf16[64,16,64]{2,1,0:T(8,128)(2,1)S(1)}, bf16[64,16,64]{2,1,0:T(8,128)(2,1)}, u32[]{:S(2)}) copy-start(bf16[64,16,64]{2,1,0:T(8,128)(2,1)} %param.35) | copy-start | bytes 393220
  6.9 0.9 %copy-start.7 = (bf16[64,1024]{1,0:T(8,128)(2,1)S(1)}, bf16[64,1024]{1,0:T(8,128)(2,1)}, u32[]{:S(2)}) copy-start(bf16[64,1024]{1,0:T(8,128)(2,1)} %feed_ref.1) | copy-start | bytes 393220
  7.8 0.8 copy-start.8
  8.6 0.8 copy-start.9
  9.4 0.7 copy-start.13
  10.0 0.7 copy-start.16
  10.7 4.4 %copy-start.2 = (bf16[64,2048]{1,0:T(8,128)(2,1)S(1)}, bf16[64,2048]{1,0:T(8,128)(2,1)}, u32[]{:S(2)}) copy-start(bf16[64,2048]{1,0:T(8,128)(2,1)} %resid_ref.1) | copy-start | bytes 786436
  10.7 4.4 %copy-start.14 = (s32[64,6]{0,1:T(8,128)S(1)}, s32[64,6]{0,1:T(8,128)}, u32[]{:S(2)}) copy-start(s32[64,6]{0,1:T(8,128)} %param.42) | copy-start | bytes 4612
  10.7 4.4 %copy-start.15 = (f32[64,6]{0,1:T(8,128)S(1)}, f32[64,6]{0,1:T(8,128)}, u32[]{:S(2)}) copy-start(f32[64,6]{0,1:T(8,128)} %param.43) | copy-start | bytes 4612

commit v2 on v1

--- a/solution.py
+++ b/solution.py
@@ -14,13 +14,37 @@
 N_DEV = 128
 CAP = 4
 SLOTS = N_DEV * CAP
-STRIDE = 43
-STRIDE_INV = pow(STRIDE, -1, N_DEV)
+
+
+def send_order():
+    def length(o):
+        return sum(min(d, 4 - d) for d in (o % 4, o // 4 % 4, o // 16))
+
+    order = [0]
+    for far in sorted(range(1, 64), key=lambda o: -length(o)):
+        x, y, z = far % 4, far // 4 % 4, far // 16
+        for a, b, c in ((x, y, z), (y, z, x), (z, x, y)):
+            for sign in (1, -1):
+                image = (sign * a) % 4 + (sign * b) % 4 * 4 + (sign * c) % 4 * 16
+                if image not in order:
+                    order.append(image)
+    return tuple(2 * o + core for o in order for core in (0, 1))
+
+
+ORDER = send_order()
 GROUPS = 4
 GROUP_DEV = N_DEV // GROUPS
 GROUP_ROWS = SLOTS // GROUPS
 NT = (((1,), (1,)), ((), ()))
 TN = (((0,), (0,)), ((), ()))
+
+
+def keep(value):
+    return pltpu.with_memory_space_constraint(value, memory_space=pltpu.HBM)
+
+
+def ahead(value):
+    return pltpu.with_memory_space_constraint(value, memory_space=pltpu.VMEM)
 
 
 def split_hi_lo(value):
@@ -197,19 +221,22 @@
         compiler_params=pltpu.CompilerParams(
             dimension_semantics=("arbitrary",), vmem_limit_bytes=20 * 2**20
         ),
+        cost_estimate=pl.CostEstimate(
+            flops=4_000_000_000, bytes_accessed=6_000_000, transcendentals=100_000
+        ),
         name="state_step",
     )(
-        branch_in,
-        state_real,
-        state_imag,
-        decay_rate,
-        frequency,
-        log_step.reshape(1, 64),
-        in_re,
-        in_im,
-        out_re,
-        out_im,
-        skip_gain.reshape(1, 1024),
+        keep(branch_in),
+        keep(state_real),
+        keep(state_imag),
+        keep(decay_rate),
+        keep(frequency),
+        keep(log_step.reshape(1, 64)),
+        keep(in_re),
+        keep(in_im),
+        keep(out_re),
+        keep(out_im),
+        keep(skip_gain.reshape(1, 1024)),
     )
 
 
@@ -227,10 +254,6 @@
     y = lax.rem(me // 8 + 4 - lax.rem(off // 8, 4), 4)
     z = lax.rem(me // 32 + 4 - off // 32, 4)
     return ((z * 4 + y) * 4 + x) * 2 + core
-
-
-def offset_of(position):
-    return lax.rem(position * STRIDE, N_DEV)
 
 
 def inv_rms(v):
@@ -245,8 +268,8 @@
     out_gain_ref,
     routes_ref,
     weights_ref,
-    glu_value_hbm,
-    glu_gate_hbm,
+    glu_value,
+    glu_gate,
     e_gate_hbm,
     e_up_hbm,
     e_down_hbm,
@@ -254,8 +277,6 @@
     s_up_hbm,
     s_down_hbm,
     out_ref,
-    glu_value,
-    glu_gate,
     e_gate,
     e_up,
     e_down,
@@ -278,17 +299,23 @@
     recv_sem,
     back_send_sem,
     back_recv_sem,
+    plane_sem,
+    all_sem,
 ):
     me = lax.axis_index("ep")
     barrier = pltpu.get_barrier_semaphore()
 
-    def greet(i, carry):
-        pl.semaphore_signal(
-            barrier, inc=1, device_id=(lax.rem(me + i, N_DEV),), device_id_type=MESH
-        )
-        return carry
-
-    lax.fori_loop(1, N_DEV, greet, 0)
+    line_x = [torus_add(me, o) for o in range(1, 8)]
+    line_y = [torus_add(me, 8 * o) for o in range(1, 4)]
+    line_z = [torus_add(me, 32 * o) for o in range(1, 4)]
+
+    def greet(sem, devices):
+        for device in devices:
+            pl.semaphore_signal(
+                sem, inc=1, device_id=(device,), device_id_type=MESH
+            )
+
+    greet(barrier, line_x + line_y + line_z)
 
     loads = []
 
@@ -298,15 +325,6 @@
         loads.append(copy)
         return copy
 
-    glu_loads = []
-    for n in range(4):
-        cols = pl.ds(n * 512, 512)
-        glu_loads.append(
-            (
-                load(glu_value_hbm.at[:, cols], glu_value.at[:, cols]),
-                load(glu_gate_hbm.at[:, cols], glu_gate.at[:, cols]),
-            )
-        )
     s_loads = [load(s_gate_hbm, s_gate), load(s_up_hbm, s_up), load(s_down_hbm, s_down)]
     e_loads = [load(e_gate_hbm, e_gate), load(e_up_hbm, e_up), load(e_down_hbm, e_down)]
 
@@ -317,7 +335,9 @@
         + jnp.bitwise_and((routes >> 3) + 4 - lax.rem(me // 8, 4), 3) * 8
         + jnp.bitwise_and((routes >> 5) + 4 - me // 32, 3) * 32
     )
-    position = jnp.bitwise_and(rel * STRIDE_INV, N_DEV - 1)
+    position = jnp.zeros_like(rel)
+    for i in range(1, N_DEV):
+        position = jnp.where(rel == ORDER[i], i, position)
     row = lax.broadcasted_iota(jnp.int32, (SLOTS, 64), 0)
     row_pos = row >> 2
     row_rank = jnp.bitwise_and(row, 3).astype(F32)
@@ -338,17 +358,21 @@
     weight_hi[...] = hi
     weight_lo[...] = lo
 
+    pl.semaphore_wait(barrier, 13)
+    greet(plane_sem, line_y)
+
     act = act_ref[...]
     square = jnp.zeros((64, 1), F32)
     for n in range(4):
         cols = slice(n * 512, n * 512 + 512)
-        for copy in glu_loads[n]:
-            copy.wait()
         value_part = jnp.dot(act, glu_value[:, cols], preferred_element_type=F32)
         gate_part = jnp.dot(act, glu_gate[:, cols], preferred_element_type=F32)
         part = value_part * jax.nn.sigmoid(gate_part)
         branch[:, cols] = part
         square = square + jnp.sum(part * part, axis=-1, keepdims=True)
+        if n == 1:
+            pl.semaphore_wait(plane_sem, 3)
+            greet(all_sem, line_z)
     scale = lax.rsqrt(square * (1.0 / 2048) + EPS)
     mid = (
         resid_ref[...].astype(F32) + branch[...] * scale * mix_gain_ref[...]
@@ -362,27 +386,24 @@
         outgoing[:, cols] = jnp.dot(
             pick[...], normed[:, cols], preferred_element_type=F32
         ).astype(BF16)
-    pl.semaphore_wait(barrier, N_DEV - 1)
+    pl.semaphore_wait(all_sem, 3)
 
     def slot(i):
-        return pl.ds(pl.multiple_of(i * CAP, CAP), CAP)
+        return pl.ds(i * CAP, CAP)
 
     pltpu.make_async_copy(
         outgoing.at[slot(0), :], received.at[slot(0), :], recv_sem.at[0]
     ).start()
 
-    def send(i, carry):
+    for i in range(1, N_DEV):
         pltpu.make_async_remote_copy(
             src_ref=outgoing.at[slot(i), :],
             dst_ref=received.at[slot(i), :],
             send_sem=send_sem,
             recv_sem=recv_sem.at[i // GROUP_DEV],
-            device_id=(torus_add(me, offset_of(i)),),
+            device_id=(torus_add(me, ORDER[i]),),
             device_id_type=MESH,
         ).start()
-        return carry
-
-    lax.fori_loop(1, N_DEV, send, 0)
 
     for copy in s_loads:
         copy.wait()
@@ -400,16 +421,15 @@
         part = buffer.at[pl.ds(first, rows), :]
         pltpu.make_async_copy(part, part, sem).wait()
 
-    def back(i, carry):
+    def back(i):
         pltpu.make_async_remote_copy(
             src_ref=produced.at[slot(i), :],
             dst_ref=returned.at[slot(i), :],
             send_sem=back_send_sem,
             recv_sem=back_recv_sem.at[i // GROUP_DEV],
-            device_id=(torus_sub(me, offset_of(i)),),
+            device_id=(torus_sub(me, ORDER[i]),),
             device_id_type=MESH,
         ).start()
-        return carry
 
     def run_group(first):
         rows = pl.ds(first, GROUP_ROWS)
@@ -423,21 +443,16 @@
                 hidden, e_down[:, cols], preferred_element_type=F32
             ).astype(BF16)
 
-    wait_group(received, recv_sem.at[0], 0, GROUP_ROWS)
-    run_group(0)
-    pltpu.make_async_copy(
-        produced.at[slot(0), :], returned.at[slot(0), :], back_recv_sem.at[0]
-    ).start()
-    lax.fori_loop(1, GROUP_DEV, back, 0)
-
-    def one_group(g, carry):
-        first = pl.multiple_of(g * GROUP_ROWS, GROUP_ROWS)
-        wait_group(received, recv_sem.at[g], first, GROUP_ROWS)
-        run_group(first)
-        lax.fori_loop(g * GROUP_DEV, (g + 1) * GROUP_DEV, back, 0)
-        return carry
-
-    lax.fori_loop(1, GROUPS, one_group, 0)
+    for g in range(GROUPS):
+        wait_group(received, recv_sem.at[g], g * GROUP_ROWS, GROUP_ROWS)
+        run_group(g * GROUP_ROWS)
+        for i in range(g * GROUP_DEV, (g + 1) * GROUP_DEV):
+            if i == 0:
+                pltpu.make_async_copy(
+                    produced.at[slot(0), :], returned.at[slot(0), :], back_recv_sem.at[0]
+                ).start()
+            else:
+                back(i)
 
     def add_group(first):
         rows = pl.ds(first, GROUP_ROWS)
@@ -484,11 +499,9 @@
     return pl.pallas_call(
         expert_kernel,
         out_shape=jax.ShapeDtypeStruct((64, 2048), BF16),
-        in_specs=[vmem] * 7 + [hbm] * 8,
+        in_specs=[vmem] * 9 + [hbm] * 6,
         out_specs=vmem,
         scratch_shapes=[
-            pltpu.VMEM((1024, 2048), BF16),
-            pltpu.VMEM((1024, 2048), BF16),
             pltpu.VMEM((2048, 512), BF16),
             pltpu.VMEM((2048, 512), BF16),
             pltpu.VMEM((512, 2048), BF16),
@@ -511,9 +524,11 @@
             pltpu.SemaphoreType.DMA((GROUPS,)),
             pltpu.SemaphoreType.DMA,
             pltpu.SemaphoreType.DMA((GROUPS,)),
+            pltpu.SemaphoreType.REGULAR,
+            pltpu.SemaphoreType.REGULAR,
         ],
         compiler_params=pltpu.CompilerParams(
-            collective_id=0, has_side_effects=True, vmem_limit_bytes=52 * 2**20
+            collective_id=0, has_side_effects=True, vmem_limit_bytes=40 * 2**20
         ),
         name="experts",
     )(
@@ -524,7 +539,9 @@
         moe_out_gain.reshape(1, 2048),
         jnp.transpose(routes),
         jnp.transpose(route_weights),
-        *weights,
+        ahead(weights[0]),
+        ahead(weights[1]),
+        *map(keep, weights[2:]),
     )
 
 

time: 82.9 us -> 69.3 us (0.84)
  local copies, waits for them, and re-layouts: 10.7 us -> 0.74 us
  Pallas kernels: 70.6 us -> 67.7 us
    unnamed x35 -> x17, local copies, waits for them, and re-layouts: 10.7 us -> 0.74 us
    pallas_call x1, Pallas kernels: 66.2 us -> 60.9 us  [experts(): pl.pallas_call(expert_kernel, out_shape=jax.ShapeDtypeStruct((64, 2048),...]
    pallas_call x1, Pallas kernels: 4.41 us -> 6.74 us  [state_step(): pl.pallas_call(state_kernel, grid=(n,), out_shape=(jax.ShapeDtypeStruct((...]
where the time goes in v2:
time: 69.3 us; the launch traced here: 69.2 us
  Pallas kernels  67.7 us (98%)
  between operations  0.77 us (1%)
  local copies, waits for them, and re-layouts  0.74 us (1%)
    pallas_call x1, Pallas kernels, experts(): pl.pallas_call(expert_kernel, out_shape=jax.ShapeDtypeStruct((64, 2048),...  60.9 us
    pallas_call x1, Pallas kernels, state_step(): pl.pallas_call(state_kernel, grid=(n,), out_shape=(jax.ShapeDtypeStruct((...  6.74 us

profile of v2, /device:TPU:1, one launch (start us, length us, event | category | flops | bytes accessed | tf_op | source)
XLA Modules:
  0.0 69.2 jit_solution(4720738838688299451)
XLA Ops:
  0.6 0.0 copy-start
  0.6 0.0 copy-start.1
  0.7 0.0 copy-start.2
  0.7 0.0 copy-start.3
  0.7 0.0 copy-start.4
  0.7 0.0 copy-start.5
  0.7 0.0 copy-start.6
  0.7 0.0 copy-start.7
  0.7 6.7 %state_step.1 = (f32[64,4096]{1,0:T(8,128)}, f32[64,4096]{1,0:T(8,128)}, bf16[64,1024]{1,0:T(8,128)(2,1)S(1)}) custom-call(bf16[64,1024]{1,0:T(8,128)(2,1)} %feed_ref.1, f32[64,4096]{1,0:T(8,128)} %re_ref.1, f32[64,4096]{1,0:T(8,128)} %im_ref.1, f32[64,64]{1,0:T(8,128)} %decay_ref.1, f32[64,64]{1,0:T(8,128)} %freq_ref.1, f32[1,64]{1,0:T(1,128)} %bitcast.31, ...), custom_call_target="tpu_custom_call" | custom-call | flops 4000000000 | bytes 6000000 | tf_op jit(solution)/shard_map/state_step/pallas_call | solution.py:199
  7.5 0.0 copy-done
  7.5 0.0 copy-done.1
  7.5 0.0 copy-done.2
  7.5 0.0 copy-done.3
  7.5 0.0 copy-done.4
  7.5 0.0 copy-done.5
  7.5 0.0 copy-done.6
  7.5 0.0 copy-done.7
  7.5 60.9 %experts.1 = bf16[64,2048]{1,0:T(8,128)(2,1)S(1)} custom-call(bf16[64,1024]{1,0:T(8,128)(2,1)S(1)} %get-tuple-element.6.act_ref, bf16[64,2048]{1,0:T(8,128)(2,1)S(1)} %copy-done.2, f32[1,2048]{1,0:T(1,128)S(1)} %bitcast.18, f32[1,2048]{1,0:T(1,128)S(1)} %bitcast.19, f32[1,2048]{1,0:T(1,128)S(1)} %bitcast.20, s32[6,64]{1,0:T(8,128)S(1)} %bitcast.21, ...), custom_call_target="tpu_custom_call" | custom-call | tf_op jit(solution)/shard_map/experts/pallas_call | solution.py:499
  68.5 0.7 %copy.29 = bf16[64,2048]{1,0:T(8,128)(2,1)} copy(bf16[64,2048]{1,0:T(8,128)(2,1)S(1)} %experts.1) | data formatting | bytes 524288
Async XLA Ops:
  0.6 6.8 %copy-start = (bf16[1024,2048]{1,0:T(8,128)(2,1)S(1)}, bf16[1024,2048]{1,0:T(8,128)(2,1)}, u32[]{:S(2)}) copy-start(bf16[1024,2048]{1,0:T(8,128)(2,1)} %glu_value.1) | copy-start | bytes 12582916
  0.6 6.8 %copy-start.1 = (bf16[1024,2048]{1,0:T(8,128)(2,1)S(1)}, bf16[1024,2048]{1,0:T(8,128)(2,1)}, u32[]{:S(2)}) copy-start(bf16[1024,2048]{1,0:T(8,128)(2,1)} %glu_gate.1) | copy-start | bytes 12582916
  0.7 6.8 %copy-start.2 = (bf16[64,2048]{1,0:T(8,128)(2,1)S(1)}, bf16[64,2048]{1,0:T(8,128)(2,1)}, u32[]{:S(2)}) copy-start(bf16[64,2048]{1,0:T(8,128)(2,1)} %resid_ref.1) | copy-start | bytes 786436
  0.7 6.8 %copy-start.3 = (f32[2048]{0:T(1024)S(1)}, f32[2048]{0:T(1024)}, u32[]{:S(2)}) copy-start(f32[2048]{0:T(1024)} %param.39) | copy-start | bytes 24580
  0.7 6.8 %copy-start.4 = (f32[2048]{0:T(1024)S(1)}, f32[2048]{0:T(1024)}, u32[]{:S(2)}) copy-start(f32[2048]{0:T(1024)} %param.40) | copy-start | bytes 24580
  0.7 6.8 %copy-start.5 = (f32[2048]{0:T(1024)S(1)}, f32[2048]{0:T(1024)}, u32[]{:S(2)}) copy-start(f32[2048]{0:T(1024)} %param.41) | copy-start | bytes 24580
  0.7 6.8 %copy-start.6 = (s32[64,6]{0,1:T(8,128)S(1)}, s32[64,6]{0,1:T(8,128)}, u32[]{:S(2)}) copy-start(s32[64,6]{0,1:T(8,128)} %param.42) | copy-start | bytes 4612
  0.7 6.8 %copy-start.7 = (f32[64,6]{0,1:T(8,128)S(1)}, f32[64,6]{0,1:T(8,128)}, u32[]{:S(2)}) copy-start(f32[64,6]{0,1:T(8,128)} %param.43) | copy-start | bytes 4612

commit v3 on v2

v3 whole, which is shorter than its diff:
```python
import functools

import jax
import jax.numpy as jnp
from jax import lax
from jax.experimental import pallas as pl
from jax.experimental.pallas import tpu as pltpu
from jax.sharding import PartitionSpec as P

MESH = pl.DeviceIdType.MESH
F32 = jnp.float32
BF16 = jnp.bfloat16
EPS = 1e-06
N_DEV = 128
CAP = 4
SLOTS = N_DEV * CAP


def send_order():
    def length(o):
        return sum(min(d, 4 - d) for d in (o % 4, o // 4 % 4, o // 16))

    order = [0]
    for far in sorted(range(1, 64), key=lambda o: -length(o)):
        x, y, z = far % 4, far // 4 % 4, far // 16
        for a, b, c in ((x, y, z), (y, z, x), (z, x, y)):
            for sign in (1, -1):
                image = (sign * a) % 4 + (sign * b) % 4 * 4 + (sign * c) % 4 * 16
                if image not in order:
                    order.append(image)
    return tuple(2 * o + core for o in order for core in (0, 1))


ORDER = send_order()
GROUPS = 4
GROUP_DEV = N_DEV // GROUPS
GROUP_ROWS = SLOTS // GROUPS
NT = (((1,), (1,)), ((), ()))
TN = (((0,), (0,)), ((), ()))


def keep(value):
    return pltpu.with_memory_space_constraint(value, memory_space=pltpu.HBM)


def split_hi_lo(value):
    hi = value.astype(BF16)
    lo = (value - hi.astype(F32)).astype(BF16)
    return hi, lo


def twice(v):
    return jnp.concatenate([v, v], axis=1)


def state_constants(decay, freq, log_step):
    group = lax.broadcasted_iota(jnp.int32, (64, 64), 0)
    lane = lax.broadcasted_iota(jnp.int32, (64, 64), 1)
    column = jnp.sum(
        jnp.where(group == lane, jnp.broadcast_to(log_step, (64, 64)), 0.0),
        axis=1,
        keepdims=True,
    )
    step_size = jnp.exp(column)
    magnitude = jnp.exp(-decay * step_size)
    phase = freq * step_size
    abar_re = magnitude * jnp.cos(phase)
    abar_im = magnitude * jnp.sin(phase)
    denominator = decay * decay + freq * freq
    numer_re = abar_re - 1.0
    coef_re = (abar_im * freq - numer_re * decay) / denominator
    coef_im = (-abar_im * decay - numer_re * freq) / denominator
    return tuple(map(twice, (abar_re, abar_im, coef_re, coef_im)))


def state_block(
    b,
    constants,
    feed_ref,
    re_ref,
    im_ref,
    in_re_ref,
    in_im_ref,
    out_re_ref,
    out_im_ref,
    skip_ref,
    next_re_ref,
    next_im_ref,
    act_ref,
):
    abar_re, abar_im, coef_re, coef_im = constants
    row_group = lax.broadcasted_iota(jnp.int32, (128, 128), 0) // 16
    lane_half = lax.broadcasted_iota(jnp.int32, (128, 128), 1) // 64
    low_half = lax.broadcasted_iota(jnp.int32, (1, 128), 1) < 64
    bb_re, bb_im = [], []
    for r in range(b * 8, b * 8 + 8):
        own = slice(r * 16, r * 16 + 16)
        b_re = twice(in_re_ref[own, :].astype(F32))
        b_im = twice(in_im_ref[own, :].astype(F32))
        c_re, c_im = coef_re[r : r + 1, :], coef_im[r : r + 1, :]
        bb_re.append(c_re * b_re - c_im * b_im)
        bb_im.append(c_re * b_im + c_im * b_re)
    here = slice(b * 128, b * 128 + 128)
    o_re = twice(out_re_ref[here, :].astype(F32))
    o_im = twice(-out_im_ref[here, :].astype(F32))
    parts_re_hi, parts_re_lo = split_hi_lo(jnp.concatenate(bb_re, axis=0))
    parts_im_hi, parts_im_lo = split_hi_lo(jnp.concatenate(bb_im, axis=0))
    feed = feed_ref[:, here]
    feed_twice = twice(feed)
    readout = jnp.zeros((64, 128), F32)
    zero = jnp.zeros((128, 128), BF16)
    for q in range(4):
        mask = row_group == 2 * q + lane_half

        def block(hi, lo):
            return jnp.concatenate(
                [jnp.where(mask, hi, zero), jnp.where(mask, lo, zero)], axis=0
            )

        f_re = jnp.dot(
            feed_twice, block(parts_re_hi, parts_re_lo), preferred_element_type=F32
        )
        f_im = jnp.dot(
            feed_twice, block(parts_im_hi, parts_im_lo), preferred_element_type=F32
        )
        r0 = b * 8 + 2 * q
        a_re = jnp.where(low_half, abar_re[r0 : r0 + 1, :], abar_re[r0 + 1 : r0 + 2, :])
        a_im = jnp.where(low_half, abar_im[r0 : r0 + 1, :], abar_im[r0 + 1 : r0 + 2, :])
        lanes = slice(b * 512 + q * 128, b * 512 + q * 128 + 128)
        old_re, old_im = re_ref[:, lanes], im_ref[:, lanes]
        new_re = a_re * old_re - a_im * old_im + f_re
        new_im = a_re * old_im + a_im * old_re + f_im
        next_re_ref[:, lanes] = new_re
        next_im_ref[:, lanes] = new_im
        re_hi, re_lo = split_hi_lo(new_re)
        im_hi, im_lo = split_hi_lo(new_im)
        w = jnp.concatenate(
            [
                jnp.where(mask, o_re, 0.0).astype(BF16),
                jnp.where(mask, o_im, 0.0).astype(BF16),
            ],
            axis=1,
        )
        left = jnp.concatenate(
            [
                jnp.concatenate([re_hi, im_hi], axis=1),
                jnp.concatenate([re_lo, im_lo], axis=1),
            ],
            axis=0,
        )
        both = lax.dot_general(left, w, NT, preferred_element_type=F32)
        readout = readout + (both[:64] + both[64:])
    mixed = readout + skip_ref[:, here] * feed.astype(F32)
    act_ref[:, here] = jax.nn.gelu(mixed).astype(BF16)


def torus_add(me, off):
    core = lax.rem(me + off, 2)
    x = lax.rem(me // 2 + off // 2, 4)
    y = lax.rem(me // 8 + off // 8, 4)
    z = lax.rem(me // 32 + off // 32, 4)
    return ((z * 4 + y) * 4 + x) * 2 + core


def torus_sub(me, off):
    core = lax.rem(me + off, 2)
    x = lax.rem(me // 2 + 4 - lax.rem(off // 2, 4), 4)
    y = lax.rem(me // 8 + 4 - lax.rem(off // 8, 4), 4)
    z = lax.rem(me // 32 + 4 - off // 32, 4)
    return ((z * 4 + y) * 4 + x) * 2 + core


def inv_rms(v):
    return lax.rsqrt(jnp.mean(v * v, axis=-1, keepdims=True) + EPS)


SMALL = (
    ("log_step", (1, 64), F32),
    ("decay", (64, 64), F32),
    ("freq", (64, 64), F32),
    ("routes", (6, 64), jnp.int32),
    ("weights", (6, 64), F32),
    ("feed", (64, 1024), BF16),
    ("in_re", (1024, 64), BF16),
    ("in_im", (1024, 64), BF16),
    ("out_re", (1024, 64), BF16),
    ("out_im", (1024, 64), BF16),
    ("skip", (1, 1024), F32),
    ("resid", (64, 2048), BF16),
    ("mix_gain", (1, 2048), F32),
    ("in_gain", (1, 2048), F32),
    ("out_gain", (1, 2048), F32),
)
STATE_PARTS = 4


def layer_kernel(*refs):
    n = len(SMALL)
    small_hbm, refs = refs[:n], refs[n:]
    (
        re_hbm,
        im_hbm,
        glu_value_hbm,
        glu_gate_hbm,
        e_gate_hbm,
        e_up_hbm,
        e_down_hbm,
        s_gate_hbm,
        s_up_hbm,
        s_down_hbm,
        out_ref,
        next_re,
        next_im,
    ) = refs[:13]
    refs = refs[13:]
    small, refs = refs[:n], refs[n:]
    (
        log_step_ref,
        decay_ref,
        freq_ref,
        routes_ref,
        weights_ref,
        feed_ref,
        in_re_ref,
        in_im_ref,
        out_re_ref,
        out_im_ref,
        skip_ref,
        resid_ref,
        mix_gain_ref,
        in_gain_ref,
        out_gain_ref,
    ) = small
    (
        old_re,
        old_im,
        act_ref,
        glu_value,
        glu_gate,
        e_gate,
        e_up,
        e_down,
        s_gate,
        s_up,
        s_down,
        branch,
        resid_mid,
        normed,
        pick,
        weight_hi,
        weight_lo,
        total,
        outgoing,
        received,
        produced,
        returned,
        load_sem,
        send_sem,
        recv_sem,
        back_send_sem,
        back_recv_sem,
        plane_sem,
        all_sem,
    ) = refs
    me = lax.axis_index("ep")
    barrier = pltpu.get_barrier_semaphore()

    line_x = [torus_add(me, o) for o in range(1, 8)]
    line_y = [torus_add(me, 8 * o) for o in range(1, 4)]
    line_z = [torus_add(me, 32 * o) for o in range(1, 4)]

    def greet(sem, devices):
        for device in devices:
            pl.semaphore_signal(
                sem, inc=1, device_id=(device,), device_id_type=MESH
            )

    greet(barrier, line_x + line_y + line_z)

    loads = []

    def load(src, dst):
        copy = pltpu.make_async_copy(src, dst, load_sem.at[len(loads)])
        copy.start()
        loads.append(copy)
        return copy

    small_loads = [load(src, dst) for src, dst in zip(small_hbm, small)]
    state_loads = []
    for part in range(STATE_PARTS):
        cols = pl.ds(part * 4096 // STATE_PARTS, 4096 // STATE_PARTS)
        state_loads.append(
            (
                load(re_hbm.at[:, cols], old_re.at[:, cols]),
                load(im_hbm.at[:, cols], old_im.at[:, cols]),
            )
        )
    glu_loads = []
    for part in range(4):
        cols = pl.ds(part * 512, 512)
        glu_loads.append(
            (
                load(glu_value_hbm.at[:, cols], glu_value.at[:, cols]),
                load(glu_gate_hbm.at[:, cols], glu_gate.at[:, cols]),
            )
        )
    for copy in small_loads[:5]:
        copy.wait()
    constants = state_constants(decay_ref[...], freq_ref[...], log_step_ref[...])

    routes = routes_ref[...]
    rel = (
        jnp.bitwise_and(routes + me, 1)
        + jnp.bitwise_and((routes >> 1) + 4 - lax.rem(me // 2, 4), 3) * 2
        + jnp.bitwise_and((routes >> 3) + 4 - lax.rem(me // 8, 4), 3) * 8
        + jnp.bitwise_and((routes >> 5) + 4 - me // 32, 3) * 32
    )
    position = jnp.zeros_like(rel)
    for i in range(1, N_DEV):
        position = jnp.where(rel == ORDER[i], i, position)
    row = lax.broadcasted_iota(jnp.int32, (SLOTS, 64), 0)
    row_pos = row >> 2
    row_rank = jnp.bitwise_and(row, 3).astype(F32)
    named = jnp.zeros((SLOTS, 64), F32)
    weight = jnp.zeros((SLOTS, 64), F32)
    for k in range(6):
        hit = row_pos == position[k : k + 1, :]
        named = jnp.where(hit, 1.0, named)
        weight = jnp.where(hit, weights_ref[k : k + 1, :], weight)
    earlier = (
        lax.broadcasted_iota(jnp.int32, (64, 64), 0)
        < lax.broadcasted_iota(jnp.int32, (64, 64), 1)
    ).astype(BF16)
    rank = jnp.dot(named.astype(BF16), earlier, preferred_element_type=F32)
    chosen = rank == row_rank
    pick[...] = jnp.where(chosen, named, 0.0).astype(BF16)
    hi, lo = split_hi_lo(jnp.where(chosen, weight, 0.0))
    weight_hi[...] = hi
    weight_lo[...] = lo

    for copy in small_loads[5:]:
        copy.wait()
    for part in range(STATE_PARTS):
        for copy in state_loads[part]:
            copy.wait()
        for b in range(part * 8 // STATE_PARTS, (part + 1) * 8 // STATE_PARTS):
            state_block(
                b,
                constants,
                feed_ref,
                old_re,
                old_im,
                in_re_ref,
                in_im_ref,
                out_re_ref,
                out_im_ref,
                skip_ref,
                next_re,
                next_im,
                act_ref,
            )
        if part == 1:
            pl.semaphore_wait(barrier, 13)
            greet(plane_sem, line_y)
    pl.semaphore_wait(plane_sem, 3)
    greet(all_sem, line_z)
    s_loads = [load(s_gate_hbm, s_gate), load(s_up_hbm, s_up), load(s_down_hbm, s_down)]
    e_loads = [load(e_gate_hbm, e_gate), load(e_up_hbm, e_up), load(e_down_hbm, e_down)]

    act = act_ref[...]
    square = jnp.zeros((64, 1), F32)
    for n in range(4):
        cols = slice(n * 512, n * 512 + 512)
        for copy in glu_loads[n]:
            copy.wait()
        value_part = jnp.dot(act, glu_value[:, cols], preferred_element_type=F32)
        gate_part = jnp.dot(act, glu_gate[:, cols], preferred_element_type=F32)
        part = value_part * jax.nn.sigmoid(gate_part)
        branch[:, cols] = part
        square = square + jnp.sum(part * part, axis=-1, keepdims=True)
    scale = lax.rsqrt(square * (1.0 / 2048) + EPS)
    mid = (
        resid_ref[...].astype(F32) + branch[...] * scale * mix_gain_ref[...]
    ).astype(BF16)
    resid_mid[...] = mid
    mid = mid.astype(F32)
    normed[...] = (mid * inv_rms(mid) * in_gain_ref[...]).astype(BF16)

    def slot(i):
        return pl.ds(i * CAP, CAP)

    for g in range(GROUPS):
        rows = slice(g * GROUP_ROWS, (g + 1) * GROUP_ROWS)
        outgoing[rows, :] = jnp.dot(
            pick[rows, :], normed[...], preferred_element_type=F32
        ).astype(BF16)
        if g == 0:
            pl.semaphore_wait(all_sem, 3)
            pltpu.make_async_copy(
                outgoing.at[slot(0), :], received.at[slot(0), :], recv_sem.at[0]
            ).start()
        for i in range(max(1, g * GROUP_DEV), (g + 1) * GROUP_DEV):
            pltpu.make_async_remote_copy(
                src_ref=outgoing.at[slot(i), :],
                dst_ref=received.at[slot(i), :],
                send_sem=send_sem,
                recv_sem=recv_sem.at[g],
                device_id=(torus_add(me, ORDER[i]),),
                device_id_type=MESH,
            ).start()

    for copy in s_loads:
        copy.wait()
    x = normed[...]
    g = jnp.dot(x, s_gate[...], preferred_element_type=F32)
    u = jnp.dot(x, s_up[...], preferred_element_type=F32)
    hidden = (jax.nn.silu(g) * u).astype(BF16)
    for n in range(4):
        cols = slice(n * 512, n * 512 + 512)
        total[:, cols] = jnp.dot(hidden, s_down[:, cols], preferred_element_type=F32)
    for copy in e_loads:
        copy.wait()

    def wait_group(buffer, sem, first, rows):
        part = buffer.at[pl.ds(first, rows), :]
        pltpu.make_async_copy(part, part, sem).wait()

    def back(i):
        pltpu.make_async_remote_copy(
            src_ref=produced.at[slot(i), :],
            dst_ref=returned.at[slot(i), :],
            send_sem=back_send_sem,
            recv_sem=back_recv_sem.at[i // GROUP_DEV],
            device_id=(torus_sub(me, ORDER[i]),),
            device_id_type=MESH,
        ).start()

    def run_group(first):
        rows = pl.ds(first, GROUP_ROWS)
        x = received[rows, :]
        g = jnp.dot(x, e_gate[...], preferred_element_type=F32)
        u = jnp.dot(x, e_up[...], preferred_element_type=F32)
        hidden = (jax.nn.silu(g) * u).astype(BF16)
        for n in range(4):
            cols = slice(n * 512, n * 512 + 512)
            produced[rows, cols] = jnp.dot(
                hidden, e_down[:, cols], preferred_element_type=F32
            ).astype(BF16)

    for g in range(GROUPS):
        wait_group(received, recv_sem.at[g], g * GROUP_ROWS, GROUP_ROWS)
        run_group(g * GROUP_ROWS)
        for i in range(g * GROUP_DEV, (g + 1) * GROUP_DEV):
            if i == 0:
                pltpu.make_async_copy(
                    produced.at[slot(0), :], returned.at[slot(0), :], back_recv_sem.at[0]
                ).start()
            else:
                back(i)

    def add_group(first):
        rows = pl.ds(first, GROUP_ROWS)
        left = jnp.concatenate([weight_hi[rows, :], weight_lo[rows, :]], axis=1)
        for n in range(4):
            cols = slice(n * 512, n * 512 + 512)
            both = lax.dot_general(
                left, returned[rows, cols], TN, preferred_element_type=F32
            )
            total[:, cols] += both[:64] + both[64:]

    wait_group(returned, back_recv_sem.at[0], 0, GROUP_ROWS)
    add_group(0)

    def add_one(g, carry):
        first = pl.multiple_of(g * GROUP_ROWS, GROUP_ROWS)
        wait_group(returned, back_recv_sem.at[g], first, GROUP_ROWS)
        add_group(first)
        return carry

    lax.fori_loop(1, GROUPS, add_one, 0)

    combined = total[...]
    out_ref[...] = (
        resid_mid[...].astype(F32)
        + combined * inv_rms(combined) * out_gain_ref[...]
    ).astype(BF16)
    wait_group(s_gate, send_sem, 0, (SLOTS - CAP) * 4)
    wait_group(s_gate, back_send_sem, 0, (SLOTS - CAP) * 4)


def layer(small, wide):
    vmem = pl.BlockSpec(memory_space=pltpu.VMEM)
    hbm = pl.BlockSpec(memory_space=pl.ANY)
    state = pltpu.VMEM((64, 4096), F32)
    row_major = pltpu.VMEM((2048, 512), BF16)
    down = pltpu.VMEM((512, 2048), BF16)
    mixer = pltpu.VMEM((1024, 2048), BF16)
    slots = pltpu.VMEM((SLOTS, 2048), BF16)
    table = pltpu.VMEM((SLOTS, 64), BF16)
    dma = pltpu.SemaphoreType.DMA
    return pl.pallas_call(
        layer_kernel,
        out_shape=(
            jax.ShapeDtypeStruct((64, 2048), BF16),
            jax.ShapeDtypeStruct((64, 4096), F32),
            jax.ShapeDtypeStruct((64, 4096), F32),
        ),
        in_specs=[hbm] * (len(small) + len(wide)),
        out_specs=(vmem, vmem, vmem),
        scratch_shapes=[pltpu.VMEM(shape, kind) for _, shape, kind in SMALL]
        + [
            state,
            state,
            pltpu.VMEM((64, 1024), BF16),
            mixer,
            mixer,
            row_major,
            row_major,
            down,
            row_major,
            row_major,
            down,
            pltpu.VMEM((64, 2048), F32),
            pltpu.VMEM((64, 2048), BF16),
            pltpu.VMEM((64, 2048), BF16),
            table,
            table,
            table,
            pltpu.VMEM((64, 2048), F32),
            slots,
            slots,
            slots,
            slots,
            dma((len(SMALL) + 2 * STATE_PARTS + 14,)),
            dma,
            dma((GROUPS,)),
            dma,
            dma((GROUPS,)),
            pltpu.SemaphoreType.REGULAR,
            pltpu.SemaphoreType.REGULAR,
        ],
        compiler_params=pltpu.CompilerParams(
            collective_id=0, has_side_effects=True, vmem_limit_bytes=42 * 2**20
        ),
        name="layer",
    )(*map(keep, small), *map(keep, wide))


def store_kernel(out_vmem, re_vmem, im_vmem, out_ref, re_ref, im_ref, sem):
    copies = [
        pltpu.make_async_copy(src, dst, sem.at[i])
        for i, (src, dst) in enumerate(
            ((re_vmem, re_ref), (im_vmem, im_ref), (out_vmem, out_ref))
        )
    ]
    for copy in copies:
        copy.start()
    for copy in copies:
        copy.wait()


def store(*arrays):
    return pl.pallas_call(
        store_kernel,
        out_shape=tuple(jax.ShapeDtypeStruct(a.shape, a.dtype) for a in arrays),
        in_specs=[pl.BlockSpec(memory_space=pltpu.VMEM)] * 3,
        out_specs=(pl.BlockSpec(memory_space=pl.ANY),) * 3,
        scratch_shapes=[pltpu.SemaphoreType.DMA((3,))],
        compiler_params=pltpu.CompilerParams(vmem_limit_bytes=2**20),
        name="store",
    )(*arrays)


def per_device(
    residual,
    branch_in,
    state_real,
    state_imag,
    decay_rate,
    frequency,
    log_step,
    input_real,
    input_imag,
    output_matrix_real,
    output_matrix_imaginary,
    skip_gain,
    glu_value,
    glu_gate,
    mix_gain,
    moe_in_gain,
    moe_out_gain,
    routes,
    route_weights,
    expert_gate,
    expert_up,
    expert_down,
    shared_gate,
    shared_up,
    shared_down,
):
    small = (
        log_step.reshape(1, 64),
        decay_rate,
        frequency,
        jnp.transpose(routes),
        jnp.transpose(route_weights),
        branch_in,
        jnp.transpose(input_real, (0, 2, 1)).reshape(1024, 64),
        jnp.transpose(input_imag, (0, 2, 1)).reshape(1024, 64),
        output_matrix_real.reshape(1024, 64),
        output_matrix_imaginary.reshape(1024, 64),
        skip_gain.reshape(1, 1024),
        residual,
        mix_gain.reshape(1, 2048),
        moe_in_gain.reshape(1, 2048),
        moe_out_gain.reshape(1, 2048),
    )
    wide = (
        state_real,
        state_imag,
        glu_value,
        glu_gate,
        expert_gate.reshape(2048, 512),
        expert_up.reshape(2048, 512),
        expert_down.reshape(512, 2048),
        shared_gate,
        shared_up,
        shared_down,
    )
    return store(*layer(small, wide))


def solution(mesh):
    return jax.shard_map(
        per_device,
        mesh=mesh,
        in_specs=(
            P("ep", None),
            P("ep", None),
            P("ep", None),
            P("ep", None),
            P(),
            P(),
            P(),
            P(),
            P(),
            P(),
            P(),
            P(),
            P(),
            P(),
            P(),
            P(),
            P(),
            P("ep", None),
            P("ep", None),
            P("ep", None, None),
            P("ep", None, None),
            P("ep", None, None),
            P(),
            P(),
            P(),
        ),
        out_specs=(P("ep", None), P("ep", None), P("ep", None)),
        check_vma=False,
    )
```

time: 69.3 us -> 65.8 us (0.949)
  Pallas kernels: 67.7 us -> 65 us
  local copies, waits for them, and re-layouts: 0.74 us -> 0 us
    pallas_call x2, Pallas kernels: 67.7 us -> 65 us  [the longest x1 63.6 us: layer(): pl.pallas_call(layer_kernel, out_shape=(jax.ShapeDtypeStruct((64, 2048),...]
    unnamed x17 -> x0, local copies, waits for them, and re-layouts: 0.74 us -> none
where the time goes in v3:
time: 65.8 us; the launch traced here: 65.7 us
  Pallas kernels  65 us (99%)
    pallas_call x1, Pallas kernels, layer(): pl.pallas_call(layer_kernel, out_shape=(jax.ShapeDtypeStruct((64, 2048),...  63.6 us
    pallas_call x1, Pallas kernels, store(): pl.pallas_call(store_kernel, out_shape=tuple((jax.ShapeDtypeStruct(a.shap...  1.42 us

profile of v3, /device:TPU:1, one launch (start us, length us, event | category | flops | bytes accessed | tf_op | source)
XLA Modules:
  0.0 65.7 jit_solution(15727996157634132571)
XLA Ops:
  0.6 63.6 %layer.1 = (bf16[64,2048]{1,0:T(8,128)(2,1)S(1)}, f32[64,4096]{1,0:T(8,128)S(1)}, f32[64,4096]{1,0:T(8,128)S(1)}) custom-call(f32[1,64]{1,0:T(1,128)} %bitcast.31, f32[64,64]{1,0:T(8,128)} %refs_1_.1, f32[64,64]{1,0:T(8,128)} %refs_2_.1, s32[6,64]{1,0:T(8,128)} %bitcast.28, f32[6,64]{1,0:T(8,128)} %bitcast.29, bf16[64,1024]{1,0:T(8,128)(2,1)} %refs_5_.1, ...), custom_call_target="tpu_custom_call" | custom-call | tf_op jit(solution)/shard_map/layer/pallas_call | solution.py:501
  64.2 1.4 %store.1 = (bf16[64,2048]{1,0:T(8,128)(2,1)}, f32[64,4096]{1,0:T(8,128)}, f32[64,4096]{1,0:T(8,128)}) custom-call(bf16[64,2048]{1,0:T(8,128)(2,1)S(1)} %get-tuple-element.6.out_vmem, f32[64,4096]{1,0:T(8,128)S(1)} %get-tuple-element.7.re_vmem, f32[64,4096]{1,0:T(8,128)S(1)} %get-tuple-element.8.im_vmem), custom_call_target="tpu_custom_call" | custom-call | tf_op jit(solution)/shard_map/store/pallas_call | solution.py:563

commit v4 on v3

--- a/solution.py
+++ b/solution.py
@@ -73,25 +73,8 @@
     return tuple(map(twice, (abar_re, abar_im, coef_re, coef_im)))
 
 
-def state_block(
-    b,
-    constants,
-    feed_ref,
-    re_ref,
-    im_ref,
-    in_re_ref,
-    in_im_ref,
-    out_re_ref,
-    out_im_ref,
-    skip_ref,
-    next_re_ref,
-    next_im_ref,
-    act_ref,
-):
-    abar_re, abar_im, coef_re, coef_im = constants
-    row_group = lax.broadcasted_iota(jnp.int32, (128, 128), 0) // 16
-    lane_half = lax.broadcasted_iota(jnp.int32, (128, 128), 1) // 64
-    low_half = lax.broadcasted_iota(jnp.int32, (1, 128), 1) < 64
+def forcing_block(b, constants, masks, feed_ref, in_re_ref, in_im_ref, next_re, next_im):
+    coef_re, coef_im = constants[2:]
     bb_re, bb_im = [], []
     for r in range(b * 8, b * 8 + 8):
         own = slice(r * 16, r * 16 + 16)
@@ -100,57 +83,66 @@
         c_re, c_im = coef_re[r : r + 1, :], coef_im[r : r + 1, :]
         bb_re.append(c_re * b_re - c_im * b_im)
         bb_im.append(c_re * b_im + c_im * b_re)
+    feed_twice = twice(feed_ref[:, b * 128 : b * 128 + 128])
+    lanes = slice(b * 512, b * 512 + 512)
+    for parts, out_ref in ((bb_re, next_re), (bb_im, next_im)):
+        hi, lo = split_hi_lo(jnp.concatenate(parts, axis=0))
+        table = jnp.concatenate(
+            [
+                jnp.concatenate([hi * mask for mask in masks], axis=1),
+                jnp.concatenate([lo * mask for mask in masks], axis=1),
+            ],
+            axis=0,
+        )
+        out_ref[:, lanes] = jnp.dot(feed_twice, table, preferred_element_type=F32)
+
+
+def state_block(
+    b,
+    constants,
+    masks,
+    feed_ref,
+    re_ref,
+    im_ref,
+    out_re_ref,
+    out_im_ref,
+    skip_ref,
+    next_re,
+    next_im,
+    act_ref,
+):
+    abar_re, abar_im = constants[:2]
+    low_half = lax.broadcasted_iota(jnp.int32, (1, 128), 1) < 64
     here = slice(b * 128, b * 128 + 128)
-    o_re = twice(out_re_ref[here, :].astype(F32))
-    o_im = twice(-out_im_ref[here, :].astype(F32))
-    parts_re_hi, parts_re_lo = split_hi_lo(jnp.concatenate(bb_re, axis=0))
-    parts_im_hi, parts_im_lo = split_hi_lo(jnp.concatenate(bb_im, axis=0))
-    feed = feed_ref[:, here]
-    feed_twice = twice(feed)
-    readout = jnp.zeros((64, 128), F32)
-    zero = jnp.zeros((128, 128), BF16)
+    his, los = [[], []], [[], []]
     for q in range(4):
-        mask = row_group == 2 * q + lane_half
-
-        def block(hi, lo):
-            return jnp.concatenate(
-                [jnp.where(mask, hi, zero), jnp.where(mask, lo, zero)], axis=0
-            )
-
-        f_re = jnp.dot(
-            feed_twice, block(parts_re_hi, parts_re_lo), preferred_element_type=F32
-        )
-        f_im = jnp.dot(
-            feed_twice, block(parts_im_hi, parts_im_lo), preferred_element_type=F32
-        )
         r0 = b * 8 + 2 * q
         a_re = jnp.where(low_half, abar_re[r0 : r0 + 1, :], abar_re[r0 + 1 : r0 + 2, :])
         a_im = jnp.where(low_half, abar_im[r0 : r0 + 1, :], abar_im[r0 + 1 : r0 + 2, :])
         lanes = slice(b * 512 + q * 128, b * 512 + q * 128 + 128)
         old_re, old_im = re_ref[:, lanes], im_ref[:, lanes]
-        new_re = a_re * old_re - a_im * old_im + f_re
-        new_im = a_re * old_im + a_im * old_re + f_im
-        next_re_ref[:, lanes] = new_re
-        next_im_ref[:, lanes] = new_im
-        re_hi, re_lo = split_hi_lo(new_re)
-        im_hi, im_lo = split_hi_lo(new_im)
-        w = jnp.concatenate(
-            [
-                jnp.where(mask, o_re, 0.0).astype(BF16),
-                jnp.where(mask, o_im, 0.0).astype(BF16),
-            ],
-            axis=1,
-        )
-        left = jnp.concatenate(
-            [
-                jnp.concatenate([re_hi, im_hi], axis=1),
-                jnp.concatenate([re_lo, im_lo], axis=1),
-            ],
-            axis=0,
-        )
-        both = lax.dot_general(left, w, NT, preferred_element_type=F32)
-        readout = readout + (both[:64] + both[64:])
-    mixed = readout + skip_ref[:, here] * feed.astype(F32)
+        new_re = a_re * old_re - a_im * old_im + next_re[:, lanes]
+        new_im = a_re * old_im + a_im * old_re + next_im[:, lanes]
+        next_re[:, lanes] = new_re
+        next_im[:, lanes] = new_im
+        for i, new in enumerate((new_re, new_im)):
+            hi, lo = split_hi_lo(new)
+            his[i].append(hi)
+            los[i].append(lo)
+    o_re = twice(out_re_ref[here, :].astype(F32)).astype(BF16)
+    o_im = twice(-out_im_ref[here, :].astype(F32)).astype(BF16)
+    w = jnp.concatenate(
+        [o_re * mask for mask in masks] + [o_im * mask for mask in masks], axis=1
+    )
+    left = jnp.concatenate(
+        [
+            jnp.concatenate(his[0] + his[1], axis=1),
+            jnp.concatenate(los[0] + los[1], axis=1),
+        ],
+        axis=0,
+    )
+    both = lax.dot_general(left, w, NT, preferred_element_type=F32)
+    mixed = both[:64] + both[64:] + skip_ref[:, here] * feed_ref[:, here].astype(F32)
     act_ref[:, here] = jax.nn.gelu(mixed).astype(BF16)
 
 
@@ -259,14 +251,12 @@
         recv_sem,
         back_send_sem,
         back_recv_sem,
-        plane_sem,
         all_sem,
     ) = refs
     me = lax.axis_index("ep")
     barrier = pltpu.get_barrier_semaphore()
 
-    line_x = [torus_add(me, o) for o in range(1, 8)]
-    line_y = [torus_add(me, 8 * o) for o in range(1, 4)]
+    plane = [torus_add(me, o) for o in range(1, 32)]
     line_z = [torus_add(me, 32 * o) for o in range(1, 4)]
 
     def greet(sem, devices):
@@ -275,7 +265,7 @@
                 sem, inc=1, device_id=(device,), device_id_type=MESH
             )
 
-    greet(barrier, line_x + line_y + line_z)
+    greet(barrier, plane + line_z)
 
     loads = []
 
@@ -295,15 +285,14 @@
                 load(im_hbm.at[:, cols], old_im.at[:, cols]),
             )
         )
-    glu_loads = []
-    for part in range(4):
-        cols = pl.ds(part * 512, 512)
-        glu_loads.append(
-            (
-                load(glu_value_hbm.at[:, cols], glu_value.at[:, cols]),
-                load(glu_gate_hbm.at[:, cols], glu_gate.at[:, cols]),
-            )
-        )
+    value_load = load(glu_value_hbm, glu_value)
+    gate_load = load(glu_gate_hbm, glu_gate)
+    row_group = lax.broadcasted_iota(jnp.int32, (128, 128), 0) // 16
+    lane_half = lax.broadcasted_iota(jnp.int32, (128, 128), 1) // 64
+    masks = [
+        jnp.where(row_group == 2 * q + lane_half, 1.0, 0.0).astype(BF16)
+        for q in range(4)
+    ]
     for copy in small_loads[:5]:
         copy.wait()
     constants = state_constants(decay_ref[...], freq_ref[...], log_step_ref[...])
@@ -340,6 +329,10 @@
 
     for copy in small_loads[5:]:
         copy.wait()
+    for b in range(8):
+        forcing_block(
+            b, constants, masks, feed_ref, in_re_ref, in_im_ref, next_re, next_im
+        )
     for part in range(STATE_PARTS):
         for copy in state_loads[part]:
             copy.wait()
@@ -347,11 +340,10 @@
             state_block(
                 b,
                 constants,
+                masks,
                 feed_ref,
                 old_re,
                 old_im,
-                in_re_ref,
-                in_im_ref,
                 out_re_ref,
                 out_im_ref,
                 skip_ref,
@@ -360,22 +352,22 @@
                 act_ref,
             )
         if part == 1:
-            pl.semaphore_wait(barrier, 13)
-            greet(plane_sem, line_y)
-    pl.semaphore_wait(plane_sem, 3)
-    greet(all_sem, line_z)
+            pl.semaphore_wait(barrier, 34)
+            greet(all_sem, line_z)
     s_loads = [load(s_gate_hbm, s_gate), load(s_up_hbm, s_up), load(s_down_hbm, s_down)]
     e_loads = [load(e_gate_hbm, e_gate), load(e_up_hbm, e_up), load(e_down_hbm, e_down)]
 
     act = act_ref[...]
     square = jnp.zeros((64, 1), F32)
+    value_load.wait()
     for n in range(4):
         cols = slice(n * 512, n * 512 + 512)
-        for copy in glu_loads[n]:
-            copy.wait()
-        value_part = jnp.dot(act, glu_value[:, cols], preferred_element_type=F32)
+        branch[:, cols] = jnp.dot(act, glu_value[:, cols], preferred_element_type=F32)
+    gate_load.wait()
+    for n in range(4):
+        cols = slice(n * 512, n * 512 + 512)
         gate_part = jnp.dot(act, glu_gate[:, cols], preferred_element_type=F32)
-        part = value_part * jax.nn.sigmoid(gate_part)
+        part = branch[:, cols] * jax.nn.sigmoid(gate_part)
         branch[:, cols] = part
         square = square + jnp.sum(part * part, axis=-1, keepdims=True)
     scale = lax.rsqrt(square * (1.0 / 2048) + EPS)
@@ -536,7 +528,6 @@
             dma((GROUPS,)),
             dma,
             dma((GROUPS,)),
-            pltpu.SemaphoreType.REGULAR,
             pltpu.SemaphoreType.REGULAR,
         ],
         compiler_params=pltpu.CompilerParams(

time: 65.8 us -> 65 us (0.988)
  Pallas kernels: 65 us -> 64.2 us
    pallas_call x1, Pallas kernels: 63.6 us -> 62.8 us  [layer(): pl.pallas_call(layer_kernel, out_shape=(jax.ShapeDtypeStruct((64, 2048),...]
where the time goes in v4:
time: 65 us; the launch traced here: 64.9 us
  Pallas kernels  64.2 us (99%)
  between operations  0.65 us (1%)
    pallas_call x1, Pallas kernels, layer(): pl.pallas_call(layer_kernel, out_shape=(jax.ShapeDtypeStruct((64, 2048),...  62.8 us
    pallas_call x1, Pallas kernels, store(): pl.pallas_call(store_kernel, out_shape=tuple((jax.ShapeDtypeStruct(a.shap...  1.42 us

profile of v4, /device:TPU:1, one launch (start us, length us, event | category | flops | bytes accessed | tf_op | source)
XLA Modules:
  0.0 64.9 jit_solution(12576436068645550996)
XLA Ops:
  0.6 62.8 %layer.1 = (bf16[64,2048]{1,0:T(8,128)(2,1)S(1)}, f32[64,4096]{1,0:T(8,128)S(1)}, f32[64,4096]{1,0:T(8,128)S(1)}) custom-call(f32[1,64]{1,0:T(1,128)} %bitcast.31, f32[64,64]{1,0:T(8,128)} %refs_1_.1, f32[64,64]{1,0:T(8,128)} %refs_2_.1, s32[6,64]{1,0:T(8,128)} %bitcast.28, f32[6,64]{1,0:T(8,128)} %bitcast.29, bf16[64,1024]{1,0:T(8,128)(2,1)} %refs_5_.1, ...), custom_call_target="tpu_custom_call" | custom-call | tf_op jit(solution)/shard_map/layer/pallas_call | solution.py:493
  63.5 1.4 %store.1 = (bf16[64,2048]{1,0:T(8,128)(2,1)}, f32[64,4096]{1,0:T(8,128)}, f32[64,4096]{1,0:T(8,128)}) custom-call(bf16[64,2048]{1,0:T(8,128)(2,1)S(1)} %get-tuple-element.6.out_vmem, f32[64,4096]{1,0:T(8,128)S(1)} %get-tuple-element.7.re_vmem, f32[64,4096]{1,0:T(8,128)S(1)} %get-tuple-element.8.im_vmem), custom_call_target="tpu_custom_call" | custom-call | tf_op jit(solution)/shard_map/store/pallas_call | solution.py:554

commit v5 on v4

--- a/solution.py
+++ b/solution.py
@@ -183,7 +183,7 @@
     ("in_gain", (1, 2048), F32),
     ("out_gain", (1, 2048), F32),
 )
-STATE_PARTS = 4
+STATE_PARTS = 2
 
 
 def layer_kernel(*refs):
@@ -238,6 +238,7 @@
         branch,
         resid_mid,
         normed,
+        slot_position,
         pick,
         weight_hi,
         weight_lo,
@@ -311,11 +312,8 @@
     row_pos = row >> 2
     row_rank = jnp.bitwise_and(row, 3).astype(F32)
     named = jnp.zeros((SLOTS, 64), F32)
-    weight = jnp.zeros((SLOTS, 64), F32)
     for k in range(6):
-        hit = row_pos == position[k : k + 1, :]
-        named = jnp.where(hit, 1.0, named)
-        weight = jnp.where(hit, weights_ref[k : k + 1, :], weight)
+        named = jnp.where(row_pos == position[k : k + 1, :], 1.0, named)
     earlier = (
         lax.broadcasted_iota(jnp.int32, (64, 64), 0)
         < lax.broadcasted_iota(jnp.int32, (64, 64), 1)
@@ -323,9 +321,7 @@
     rank = jnp.dot(named.astype(BF16), earlier, preferred_element_type=F32)
     chosen = rank == row_rank
     pick[...] = jnp.where(chosen, named, 0.0).astype(BF16)
-    hi, lo = split_hi_lo(jnp.where(chosen, weight, 0.0))
-    weight_hi[...] = hi
-    weight_lo[...] = lo
+    slot_position[...] = position
 
     for copy in small_loads[5:]:
         copy.wait()
@@ -351,7 +347,7 @@
                 next_im,
                 act_ref,
             )
-        if part == 1:
+        if part == 0:
             pl.semaphore_wait(barrier, 34)
             greet(all_sem, line_z)
     s_loads = [load(s_gate_hbm, s_gate), load(s_up_hbm, s_up), load(s_down_hbm, s_down)]
@@ -401,6 +397,13 @@
                 device_id_type=MESH,
             ).start()
 
+    weight = jnp.zeros((SLOTS, 64), F32)
+    for k in range(6):
+        hit = row_pos == slot_position[k : k + 1, :]
+        weight = jnp.where(hit, weights_ref[k : k + 1, :], weight)
+    hi, lo = split_hi_lo(weight * pick[...].astype(F32))
+    weight_hi[...] = hi
+    weight_lo[...] = lo
     for copy in s_loads:
         copy.wait()
     x = normed[...]
@@ -515,6 +518,7 @@
             pltpu.VMEM((64, 2048), F32),
             pltpu.VMEM((64, 2048), BF16),
             pltpu.VMEM((64, 2048), BF16),
+            pltpu.VMEM((6, 64), jnp.int32),
             table,
             table,
             table,

time: 65 us -> 64.8 us (level)
  no operation moved by 1% of the time
where the time goes in v5:
time: 64.8 us; the launch traced here: 64.7 us
  Pallas kernels  64.1 us (99%)
  between operations  0.65 us (1%)
    pallas_call x1, Pallas kernels, layer(): pl.pallas_call(layer_kernel, out_shape=(jax.ShapeDtypeStruct((64, 2048),...  62.7 us
    pallas_call x1, Pallas kernels, store(): pl.pallas_call(store_kernel, out_shape=tuple((jax.ShapeDtypeStruct(a.shap...  1.42 us

profile of v5, /device:TPU:1, one launch (start us, length us, event | category | flops | bytes accessed | tf_op | source)
XLA Modules:
  0.0 64.7 jit_solution(3949817721132485403)
XLA Ops:
  0.6 62.7 %layer.1 = (bf16[64,2048]{1,0:T(8,128)(2,1)S(1)}, f32[64,4096]{1,0:T(8,128)S(1)}, f32[64,4096]{1,0:T(8,128)S(1)}) custom-call(f32[1,64]{1,0:T(1,128)} %bitcast.31, f32[64,64]{1,0:T(8,128)} %refs_1_.1, f32[64,64]{1,0:T(8,128)} %refs_2_.1, s32[6,64]{1,0:T(8,128)} %bitcast.28, f32[6,64]{1,0:T(8,128)} %bitcast.29, bf16[64,1024]{1,0:T(8,128)(2,1)} %refs_5_.1, ...), custom_call_target="tpu_custom_call" | custom-call | tf_op jit(solution)/shard_map/layer/pallas_call | solution.py:496
  63.3 1.4 %store.1 = (bf16[64,2048]{1,0:T(8,128)(2,1)}, f32[64,4096]{1,0:T(8,128)}, f32[64,4096]{1,0:T(8,128)}) custom-call(bf16[64,2048]{1,0:T(8,128)(2,1)S(1)} %get-tuple-element.6.out_vmem, f32[64,4096]{1,0:T(8,128)S(1)} %get-tuple-element.7.re_vmem, f32[64,4096]{1,0:T(8,128)S(1)} %get-tuple-element.8.im_vmem), custom_call_target="tpu_custom_call" | custom-call | tf_op jit(solution)/shard_map/store/pallas_call | solution.py:558
